TPU v7x, 512 devices: a 4x2x32 block of a 4x8x32 slice. The times are simulated.
512 devices in a mesh: grp: 2 (over y), kv: 32 (over z), tp: 8 (over x, core).
Axes of the slice: x: 4, y: 2, z: 32, core: 2. Of those that a mesh axis runs over, the one named last changes fastest.
The devices are a block of a 4x8x32 slice.
Arguments:
- tokens: bfloat16 [256, 4096], P('grp', 'kv'), parts along dimension 0, may hold values from -40 to 40
- lengths: int32 [256], P(('grp', 'kv')), parts along dimension 0, may hold values from 1 to 6, 320 in all
- conv_state_x: bfloat16 [256, 3, 4096], P(('grp', 'kv'), None, 'tp'), parts along dimension 0, may hold values from -6 to 6
- conv_state_bc: bfloat16 [256, 3, 2, 1024], P(('grp', 'kv'), None, None, 'tp'), parts along dimension 0, may hold values from -6 to 6
- ssm_state: float32 [256, 64, 64, 128], P(('grp', 'kv'), 'tp'), parts along dimension 0, may hold values from -0.6 to 0.6
- norm_gain: bfloat16 [4096], P('kv'), may hold values from 0.099609375 to 1.8984375
- w_gate: bfloat16 [4096, 4096], P('kv', 'tp'), may hold values from -0.09375 to 0.09375
- w_value: bfloat16 [4096, 4096], P('kv', 'tp'), may hold values from -0.09375 to 0.09375
- w_key: bfloat16 [4096, 1024], P('kv', 'tp'), may hold values from -0.09375 to 0.09375
- w_query: bfloat16 [4096, 1024], P('kv', 'tp'), may hold values from -0.09375 to 0.09375
- w_step: bfloat16 [4096, 64], P('kv', 'tp'), may hold values from -0.09375 to 0.09375
- step_bias: float32 [64], P('tp'), may hold values from -2 to 0
- decay_log: float32 [64], P('tp'), may hold values from -2 to 1
- conv_x: bfloat16 [4, 4096], P(None, 'tp'), may hold values from -3 to 3
- conv_bc: bfloat16 [4, 2, 1024], P(None, None, 'tp'), may hold values from -3 to 3
- inner_gain: bfloat16 [4096], P('tp'), may hold values from 0.099609375 to 1.8984375
- w_out: bfloat16 [4096, 4096], P('tp', 'kv'), may hold values from -0.09375 to 0.09375
- mlp_gain: bfloat16 [4096], P('kv'), may hold values from 0.099609375 to 1.8984375
- w_up: bfloat16 [4096, 16384], P('kv', 'tp'), may hold values from -0.09375 to 0.09375
- w_down: bfloat16 [16384, 4096], P('tp', 'kv'), may hold values from -0.046875 to 0.046875
Outputs:
- layer_out: bfloat16 [256, 4096], P('grp', 'kv'), parts along dimension 0
- next_state: float32 [256, 64, 64, 128], P(('grp', 'kv'), 'tp'), parts along dimension 0
There are 2 independent parts, one for each index of `grp`. A program takes and returns all parts, laid end to end along the dimension named above; an argument that names none is the same for every part. Nothing has to cross between parts.
All inputs are finite; a program needn't handle non-finite values. No bound on the sum of `lengths` on one device may be relied on, other than what follows from the above.
Results may differ from a plain program's by a relative error of at most 0.008.
Values may be sent and summed in bfloat16 or wider, within the bound.
No kernel may reach another device: no remote copies, remote signals or barrier semaphores. Data moves between devices by JAX's collectives and lax.ppermute only.
A program may use at most 64 MiB of HBM per device.

v0:
```python
import functools

import jax
import jax.numpy as jnp
from jax import lax
from jax.experimental import pallas as pl
from jax.sharding import Mesh, PartitionSpec as P


HEAD_DIM = 64
STATE = 128
CONV_WIDTH = 4
LANES = 128
NEAR = 4

epsilon = 1e-06
f32, bf16 = jnp.float32, jnp.bfloat16


def scattered_sum(rows, along):
    size = lax.axis_size(along)
    parts = rows.reshape(size, -1, rows.shape[1])
    return lax.all_to_all(parts, along, 0, 0, tiled=True).astype(f32).sum(axis=0)


def from_everyone(shard, along):
    copies = jnp.broadcast_to(shard, (lax.axis_size(along), *shard.shape))
    return lax.all_to_all(copies, along, 0, 0, tiled=True)


def in_turn(packed, here):
    near = packed.shape[0]
    pieces = []
    for step in range(near):
        piece = lax.dynamic_index_in_dim(packed, here ^ step, keepdims=False)
        if step:
            piece = lax.ppermute(piece, "near", [(i, i ^ step) for i in range(near)])
        pieces.append(piece)
    pieces = jnp.stack(pieces)
    return jnp.stack(
        [lax.dynamic_index_in_dim(pieces, here ^ i, keepdims=False) for i in range(near)]
    )


def hi_lo(column):
    hi = column.astype(bf16)
    lo = (column - hi.astype(f32)).astype(bf16)
    lane = lax.broadcasted_iota(jnp.int32, (column.shape[0], LANES), 1)
    return jnp.where(lane == 0, hi, jnp.where(lane == 1, lo, jnp.zeros((), bf16)))


def project_kernel(
    far, near, seqs, tokens_ref, gain_ref, gate_ref, value_ref, key_ref, query_ref, step_ref, sent_ref, rows_ref
):
    batch, width = tokens_ref.shape
    to = lax.broadcasted_iota(jnp.int32, (batch, batch), 0)
    at = lax.broadcasted_iota(jnp.int32, (batch, batch), 1)
    group = to // (far * seqs)
    rest = to - group * (far * seqs)
    block = rest // seqs
    source = (block * near + group) * seqs + rest - block * seqs
    order = jnp.where(at == source, 1.0, 0.0).astype(bf16)
    wide = product(order, tokens_ref[...])
    scaled = (wide * gain_ref[...].astype(f32)).astype(bf16)
    column = 0
    for weight in (gate_ref, value_ref, key_ref, query_ref):
        size = weight.shape[1]
        sent_ref[:, column : column + size] = product(scaled, weight[...]).astype(bf16)
        column += size
    heads = step_ref.shape[0]
    steps = jnp.concatenate(
        [step_ref[...].astype(f32), jnp.zeros((LANES - heads, width), f32)], axis=0
    ).astype(bf16)
    steps = lax.dot_general(
        scaled, steps, (((1,), (1,)), ((), ())), preferred_element_type=f32
    )
    squares = jnp.sum(wide * wide, axis=1, keepdims=True)
    high = squares.astype(bf16).astype(f32)
    lane = lax.broadcasted_iota(jnp.int32, (batch, LANES), 1)
    steps = jnp.where(lane == heads, high, jnp.where(lane == heads + 1, squares - high, steps))
    sent_ref[:, column:] = steps.astype(bf16)
    rows_ref[...] = wide.astype(bf16)


def project(tokens, norm_gain, w_gate, w_value, w_key, w_query, w_step, far, near):
    batch, width = tokens.shape
    columns = sum(w.shape[1] for w in (w_gate, w_value, w_key, w_query)) + LANES
    return pl.pallas_call(
        functools.partial(project_kernel, far, near, batch // (far * near)),
        out_shape=(
            jax.ShapeDtypeStruct((batch, columns), bf16),
            jax.ShapeDtypeStruct((batch, width), bf16),
        ),
        cost_estimate=pl.CostEstimate(
            flops=2 * batch * width * columns,
            bytes_accessed=2 * columns * (batch + width),
            transcendentals=0,
        ),
        name="project",
    )(tokens, norm_gain[None], w_gate, w_value, w_key, w_query, w_step.T)


def causal_conv(state_rows, newest, conv_weights):
    extended = jnp.concatenate([state_rows, newest[:, None]], axis=1)
    conv_sum = extended[:, 0] * conv_weights[0].astype(f32)
    for offset in range(1, conv_weights.shape[0]):
        conv_sum = conv_sum + extended[:, offset] * conv_weights[offset].astype(f32)
    return jax.nn.silu(conv_sum)


def product(left, right, out=f32):
    return jnp.dot(left, right, preferred_element_type=out)


def per_device(
    tokens,
    lengths,
    conv_state_x,
    conv_state_bc,
    ssm_state,
    norm_gain,
    w_gate,
    w_value,
    w_key,
    w_query,
    w_step,
    step_bias,
    decay_log,
    conv_x,
    conv_bc,
    inner_gain,
    w_out,
    mlp_gain,
    w_up,
    w_down,
):
    far, near = lax.axis_size("far"), lax.axis_size("near")
    head_count = w_step.shape[1]
    group_count = w_key.shape[1] // STATE
    per_group = head_count // group_count
    batch, width = tokens.shape
    model = width * far * near
    inner = w_gate.shape[1] * lax.axis_size("tp")
    seqs = batch // (far * near)

    sent, token_rows = project(
        tokens, norm_gain, w_gate, w_value, w_key, w_query, w_step, far, near
    )
    near_sum = scattered_sum(sent, "near").astype(bf16)
    mine = scattered_sum(near_sum, "far")

    hidden = w_up.shape[1] // near
    blocks = hidden // width
    extra = jnp.concatenate(
        [jnp.broadcast_to(mlp_gain[None], (8, width)), near_sum[:8, :width]], axis=0
    )
    packed = jnp.concatenate(
        [
            w_up.reshape(width, near, blocks, width).transpose(1, 2, 0, 3).reshape(near, -1, width),
            jnp.broadcast_to(w_out[None], (near, *w_out.shape)),
            token_rows.reshape(near, -1, width),
            jnp.broadcast_to(extra[None], (near, *extra.shape)),
        ],
        axis=1,
    )
    here = lax.axis_index("near")
    swapped = in_turn(packed, here)
    own_up = swapped[:, :hidden].reshape(near, blocks, width, width)
    own_up = own_up.transpose(0, 2, 1, 3).reshape(near * width, hidden)
    at = hidden + w_out.shape[0]
    own_out = swapped[:, hidden:at]
    near_tokens = swapped[:, at : at + batch // near].swapaxes(0, 1).reshape(-1, near * width)
    near_gain = swapped[:, at + batch // near].reshape(1, near * width).astype(f32)

    cuts, at = [], 0
    for size in (w_gate.shape[1], w_value.shape[1], w_key.shape[1], w_query.shape[1], head_count):
        cuts.append(mine[:, at : at + size])
        at += size
    gate_raw, value_raw, key_raw, query_raw, step_raw = cuts
    squares = jnp.sum(mine[:, at:], axis=1, keepdims=True)
    inverse = lax.rsqrt(squares / model + epsilon)

    row_live = (
        jnp.arange(CONV_WIDTH - 1, dtype=jnp.int32)[None, :] >= CONV_WIDTH - 1 - lengths[:, None]
    ).astype(f32)
    live_x = conv_state_x.astype(f32) * row_live[:, :, None]
    live_bc = conv_state_bc.astype(f32) * row_live[:, :, None, None]
    mixed_values = causal_conv(live_x, value_raw * inverse, conv_x).reshape(
        seqs, head_count, HEAD_DIM
    )
    key_query = causal_conv(
        live_bc, jnp.stack([key_raw * inverse, query_raw * inverse], axis=1), conv_bc
    )
    key_heads = jnp.repeat(key_query[:, 0].reshape(seqs, group_count, STATE), per_group, axis=1)
    query_heads = jnp.repeat(key_query[:, 1].reshape(seqs, group_count, STATE), per_group, axis=1)
    step_size = jax.nn.softplus(step_raw * inverse + step_bias)
    decay = jnp.exp(-jnp.exp(decay_log) * step_size)
    fed = step_size[:, :, None] * mixed_values
    overlap = jnp.sum(key_heads * query_heads, axis=2)
    mixer_y = (
        decay[:, :, None] * jnp.sum(ssm_state * query_heads[:, :, None, :], axis=3)
        + fed * overlap[:, :, None]
    ).reshape(seqs, head_count * HEAD_DIM)
    gated_rows = mixer_y * jax.nn.silu(gate_raw * inverse)
    gated_low = (gated_rows * inner_gain.astype(f32)).astype(bf16)
    gated_low, old_state = lax.optimization_barrier((gated_low, ssm_state))
    next_state = old_state * decay[:, :, None, None] + fed[:, :, :, None] * key_heads[:, :, None, :]
    picks = [here == i for i in range(near)]
    own_up, own_out, near_gain, near_tokens, next_state, picks = lax.optimization_barrier(
        (own_up, own_out, near_gain, near_tokens, next_state, picks)
    )

    all_low = from_everyone(gated_low, "far")
    all_low = all_low.reshape(far * seqs, -1)
    ungained = all_low.astype(f32) / inner_gain.astype(f32)
    gated_squares = hi_lo(jnp.sum(ungained * ungained, axis=1, keepdims=True))
    out_part = [product(all_low, own_out[i], bf16) for i in range(near)]
    shared = from_everyone(jnp.concatenate([*out_part, gated_squares], axis=1), "tp")
    shared = shared.astype(f32).sum(axis=0)
    gated_total = jnp.sum(shared[:, near * width :], axis=1, keepdims=True)
    residual = (
        near_tokens.astype(f32)
        + shared[:, : near * width] * lax.rsqrt(gated_total / inner + epsilon)
    ).astype(bf16)

    residual = from_everyone(residual, "near")
    residual = residual.reshape(batch, near * width)
    residual_wide = residual.astype(f32)
    hidden_low = (residual_wide * near_gain).astype(bf16)
    row_squares = jnp.sum(residual_wide * residual_wide, axis=1, keepdims=True)
    up_part = jnp.concatenate([product(hidden_low, own_up, bf16), hi_lo(row_squares)], axis=1)
    own_rows = residual[:, :width]
    for i in range(1, near):
        own_rows = jnp.where(picks[i], residual[:, i * width : (i + 1) * width], own_rows)
    up_part, own_rows = lax.optimization_barrier((up_part, own_rows))
    up_mine = scattered_sum(up_part, "far")
    own_down = in_turn(w_down.reshape(near, hidden, width), here)
    up_share, square_share = up_mine[:, :hidden], jnp.sum(up_mine[:, hidden:], axis=1, keepdims=True)
    active = jnp.square(
        jax.nn.relu(up_share * lax.rsqrt(square_share / model + epsilon))
    ).astype(bf16)
    active = from_everyone(active, "far")
    active = active.reshape(batch, hidden)
    down_part = jnp.stack([product(active, own_down[i], bf16) for i in range(near)])
    down_sum = lax.all_to_all(down_part, "near", 0, 0, tiled=True).astype(f32).sum(axis=0)
    down_sum = from_everyone(down_sum.astype(bf16), "tp").astype(f32).sum(axis=0)
    finished = (own_rows.astype(f32) + down_sum).astype(bf16).reshape(near, far, seqs, width)
    return (finished.swapaxes(0, 1).reshape(batch, width), next_state)


def solution(mesh):
    kv = mesh.shape["kv"]
    near = NEAR if kv % NEAR == 0 else 1
    names = ("grp", "far", "near", "tp")
    split = Mesh(mesh.devices.reshape(mesh.shape["grp"], kv // near, near, mesh.shape["tp"]), names)
    kv = ("far", "near")
    seq = ("grp", "far", "near")
    return jax.shard_map(
        per_device,
        mesh=split,
        in_specs=(
            P("grp", kv),
            P(seq),
            P(seq, None, "tp"),
            P(seq, None, None, "tp"),
            P(seq, "tp", None, None),
            P(kv),
            P(kv, "tp"),
            P(kv, "tp"),
            P(kv, "tp"),
            P(kv, "tp"),
            P(kv, "tp"),
            P("tp"),
            P("tp"),
            P(None, "tp"),
            P(None, None, "tp"),
            P("tp"),
            P("tp", kv),
            P(kv),
            P(kv, "tp"),
            P("tp", kv),
        ),
        out_specs=(P("grp", kv), P(seq, "tp", None, None)),
        check_vma=False,
    )
```

profile of v0, /device:TPU:33, one launch (start us, length us, event | category | flops | bytes accessed | tf_op | source)
XLA Modules:
  0.0 251.7 jit_solution(9069245087166951266)
XLA Ops:
  0.6 2.2 project.1
  2.9 9.0 %all-to-all-start = ((bf16[4,32,1408]{2,1,0:T(8,128)(2,1)}), bf16[4,32,1408]{2,1,0:T(8,128)(2,1)S(1)}, u32[]{:S(2)}, u32[]{:S(2)}) async-start(bf16[4,32,1408]{2,1,0:T(8,128)(2,1)} %bitcast.194), calls=%async_computation | async-start | bytes 720896 | tf_op jit(solution)/shard_map/all_to_all | solution.py:23
  12.8 5.5 %all-to-all-done = bf16[4,32,1408]{2,1,0:T(8,128)(2,1)S(1)} async-done(((bf16[4,32,1408]{2,1,0:T(8,128)(2,1)}), bf16[4,32,1408]{2,1,0:T(8,128)(2,1)S(1)}, u32[]{:S(2)}, u32[]{:S(2)}) %all-to-all-start) | async-done | bytes 360480 | tf_op jit(solution)/shard_map/all_to_all | solution.py:23
  18.7 2.4 collective-permute-start.1
  21.1 4.8 %collective-permute-start.2 = (bf16[1072,128]{1,0:T(8,128)(2,1)S(1)}, bf16[1072,128]{1,0:T(8,128)(2,1)S(1)}, u32[]{:S(2)}, u32[]{:S(2)}) collective-permute-start(bf16[1072,128]{1,0:T(8,128)(2,1)S(1)} %get-tuple-element.41), channel_id=1, source_target_pairs={{0,24},{8,16},{16,8},{24,0},{1,25},{9,17},{17,9},{25,1},{2,26},{10... | collective-permute-start | bytes 823304 | tf_op jit(solution)/shard_map/ppermute | solution.py:37
  25.9 2.0 collective-permute-start
  28.7 43.6 %all-to-all-start.1 = ((bf16[8,4,1408]{2,1,0:T(4,128)(2,1)}), bf16[8,4,1408]{2,1,0:T(4,128)(2,1)S(1)}, u32[]{:S(2)}, u32[]{:S(2)}) async-start(bf16[8,4,1408]{2,1,0:T(4,128)(2,1)} %reshape.210), calls=%async_computation.1 | async-start | bytes 180224 | tf_op jit(solution)/shard_map/all_to_all | solution.py:23
  73.3 22.7 %all-to-all-done.1 = bf16[8,4,1408]{2,1,0:T(4,128)(2,1)S(1)} async-done(((bf16[8,4,1408]{2,1,0:T(4,128)(2,1)}), bf16[8,4,1408]{2,1,0:T(4,128)(2,1)S(1)}, u32[]{:S(2)}, u32[]{:S(2)}) %all-to-all-start.1) | async-done | bytes 90144 | tf_op jit(solution)/shard_map/all_to_all | solution.py:23
  98.2 3.5 %all-to-all-start.2 = ((bf16[8,4,512]{2,1,0:T(4,128)(2,1)}), bf16[8,4,512]{2,1,0:T(4,128)(2,1)S(1)}, u32[]{:S(2)}, u32[]{:S(2)}) async-start(bf16[8,4,512]{2,1,0:T(4,128)(2,1)} %broadcast_in_dim.55), calls=%async_computation.2 | async-start | bytes 65536 | tf_op jit(solution)/shard_map/all_to_all | solution.py:28
  101.7 1.3 multiply_add_fusion
  103.1 19.8 %all-to-all-done.2 = bf16[8,4,512]{2,1,0:T(4,128)(2,1)S(1)} async-done(((bf16[8,4,512]{2,1,0:T(4,128)(2,1)}), bf16[8,4,512]{2,1,0:T(4,128)(2,1)S(1)}, u32[]{:S(2)}, u32[]{:S(2)}) %all-to-all-start.2) | async-done | bytes 32800 | tf_op jit(solution)/shard_map/all_to_all | solution.py:28
  123.9 17.0 %all_to_all.45 = bf16[8,32,640]{2,1,0:T(8,128)(2,1)S(1)} all-to-all(bf16[8,32,640]{2,1,0:T(8,128)(2,1)S(1)} %broadcast_in_dim.59), channel_id=1, replica_groups=mesh['grp'=2,'far'=8,'near'=4,'tp'=8] {'tp'}, dimensions={0} | all-to-all | bytes 655360 | tf_op jit(solution)/shard_map/all_to_all | solution.py:28
  141.2 16.4 %all_to_all.46 = bf16[4,32,512]{2,1,0:T(8,128)(2,1)S(1)} all-to-all(bf16[4,32,512]{2,1,0:T(8,128)(2,1)S(1)} %broadcast_in_dim.60), channel_id=1, replica_groups=mesh['grp'=2,'far'=8,'near'=4,'tp'=8] {'near'}, dimensions={0} | all-to-all | bytes 262144 | tf_op jit(solution)/shard_map/all_to_all | solution.py:28
  158.2 31.2 %all_to_all.47 = bf16[8,16,640]{2,1,0:T(8,128)(2,1)S(1)} all-to-all(bf16[8,16,640]{2,1,0:T(8,128)(2,1)S(1)} %bitcast.192), channel_id=1, replica_groups=mesh['grp'=2,'far'=8,'near'=4,'tp'=8] {'far'}, dimensions={0} | all-to-all | bytes 327680 | tf_op jit(solution)/shard_map/all_to_all | solution.py:23
  189.7 0.7 broadcast_in_dim.71
  190.3 6.5 %all-to-all-start.6 = ((bf16[8,16,512]{2,1,0:T(8,128)(2,1)}), bf16[8,16,512]{2,1,0:T(8,128)(2,1)S(1)}, u32[]{:S(2)}, u32[]{:S(2)}) async-start(bf16[8,16,512]{2,1,0:T(8,128)(2,1)} %broadcast_in_dim.71), calls=%async_computation.6 | async-start | bytes 262144 | tf_op jit(solution)/shard_map/all_to_all | solution.py:28
  196.9 2.8 %collective-permute-start.3 = (bf16[512,128]{1,0:T(8,128)(2,1)S(1)}, bf16[512,128]{1,0:T(8,128)(2,1)S(1)}, u32[]{:S(2)}, u32[]{:S(2)}) collective-permute-start(bf16[512,128]{1,0:T(8,128)(2,1)S(1)} %get-tuple-element.47), channel_id=1, source_target_pairs={{0,8},{8,0},{16,24},{24,16},{1,9},{9,1},{17,25},{25,17},{2,10},{10... | collective-permute-start | bytes 393224 | tf_op jit(solution)/shard_map/ppermute | solution.py:37
  199.7 4.3 %collective-permute-start.4 = (bf16[512,128]{1,0:T(8,128)(2,1)S(1)}, bf16[512,128]{1,0:T(8,128)(2,1)S(1)}, u32[]{:S(2)}, u32[]{:S(2)}) collective-permute-start(bf16[512,128]{1,0:T(8,128)(2,1)S(1)} %get-tuple-element.46), channel_id=1, source_target_pairs={{0,16},{8,24},{16,0},{24,8},{1,17},{9,25},{17,1},{25,9},{2,18},{10... | collective-permute-start | bytes 393224 | tf_op jit(solution)/shard_map/ppermute | solution.py:37
  203.9 2.3 collective-permute-start.5
  206.2 7.0 %collective-permute-done.3 = bf16[512,128]{1,0:T(8,128)(2,1)S(1)} collective-permute-done((bf16[512,128]{1,0:T(8,128)(2,1)S(1)}, bf16[512,128]{1,0:T(8,128)(2,1)S(1)}, u32[]{:S(2)}, u32[]{:S(2)}) %collective-permute-start.3) | collective-permute-done | bytes 131104 | tf_op jit(solution)/shard_map/ppermute | solution.py:37
  213.7 6.0 %collective-permute-done.5 = bf16[512,128]{1,0:T(8,128)(2,1)S(1)} collective-permute-done((bf16[512,128]{1,0:T(8,128)(2,1)S(1)}, bf16[512,128]{1,0:T(8,128)(2,1)S(1)}, u32[]{:S(2)}, u32[]{:S(2)}) %collective-permute-start.5) | collective-permute-done | bytes 131104 | tf_op jit(solution)/shard_map/ppermute | solution.py:37
  219.9 3.0 %all-to-all-done.6 = bf16[8,16,512]{2,1,0:T(8,128)(2,1)S(1)} async-done(((bf16[8,16,512]{2,1,0:T(8,128)(2,1)}), bf16[8,16,512]{2,1,0:T(8,128)(2,1)S(1)}, u32[]{:S(2)}, u32[]{:S(2)}) %all-to-all-start.6) | async-done | bytes 131104 | tf_op jit(solution)/shard_map/all_to_all | solution.py:28
  223.7 9.5 %all_to_all.48 = bf16[4,128,128]{2,1,0:T(8,128)(2,1)S(1)} all-to-all(bf16[4,128,128]{2,1,0:T(8,128)(2,1)S(1)} %pad_maximum_fusion.5), channel_id=1, replica_groups=mesh['grp'=2,'far'=8,'near'=4,'tp'=8] {'near'}, dimensions={0} | all-to-all | bytes 262144 | tf_op jit(solution)/shard_map/all_to_all | solution.py:245
  233.3 17.7 %all_to_all.49 = bf16[8,128,128]{2,1,0:T(8,128)(2,1)S(1)} all-to-all(bf16[8,128,128]{2,1,0:T(8,128)(2,1)S(1)} %broadcast_in_dim.72), channel_id=1, replica_groups=mesh['grp'=2,'far'=8,'near'=4,'tp'=8] {'tp'}, dimensions={0} | all-to-all | bytes 524288 | tf_op jit(solution)/shard_map/all_to_all | solution.py:28
  (117 shorter events, 9.0 us)
Async XLA Ops:
  0.6 11.3 %copy-start.1 = (bf16[128,2048]{1,0:T(8,128)(2,1)S(1)}, bf16[128,2048]{1,0:T(8,128)(2,1)}, u32[]{:S(2)}) copy-start(bf16[128,2048]{1,0:T(8,128)(2,1)} %param.38) | copy-start | bytes 1572868
  2.9 15.4 %all-to-all-start = ((bf16[4,32,1408]{2,1,0:T(8,128)(2,1)}), bf16[4,32,1408]{2,1,0:T(8,128)(2,1)S(1)}, u32[]{:S(2)}, u32[]{:S(2)}) async-start(bf16[4,32,1408]{2,1,0:T(8,128)(2,1)} %bitcast.194), calls=%async_computation | async-start | bytes 720896 | tf_op jit(solution)/shard_map/all_to_all | solution.py:23
  11.9 0.7 copy-start.12
  11.9 0.8 copy-start.13
  11.9 0.8 copy-start.8
  11.9 0.8 copy-start.5
  11.9 0.8 copy-start.7
  11.9 6.4 %copy-start.10 = (bf16[128]{0:T(256)(128)(2,1)S(1)}, bf16[128]{0:T(256)(128)(2,1)}, u32[]{:S(2)}) copy-start(bf16[128]{0:T(256)(128)(2,1)} %param.37) | copy-start | bytes 772
  11.9 6.5 %copy-start.3 = (bf16[512,128]{1,0:T(8,128)(2,1)S(1)}, bf16[512,128]{1,0:T(8,128)(2,1)}, u32[]{:S(2)}) copy-start(bf16[512,128]{1,0:T(8,128)(2,1)} %param.36) | copy-start | bytes 393220
  12.2 6.3 %copy-start.4 = (bf16[128,128]{1,0:T(8,128)(2,1)S(1)}, bf16[128,128]{1,0:T(8,128)(2,1)}, u32[]{:S(2)}) copy-start(bf16[128,128]{1,0:T(8,128)(2,1)} %get-tuple-element.16) | copy-start | bytes 98308
  18.6 9.3 %copy-start.9 = (bf16[512]{0:T(512)(128)(2,1)S(1)}, bf16[512]{0:T(512)(128)(2,1)}, u32[]{:S(2)}) copy-start(bf16[512]{0:T(512)(128)(2,1)} %param.35) | copy-start | bytes 3076
  18.6 9.3 %copy-start.6 = (bf16[4,3,512]{2,0,1:T(4,128)(2,1)S(1)}, bf16[4,3,512]{2,0,1:T(4,128)(2,1)}, u32[]{:S(2)}) copy-start(bf16[4,3,512]{2,0,1:T(4,128)(2,1)} %param.22) | copy-start | bytes 36868
  18.7 53.6 %collective-permute-start.1 = (bf16[1072,128]{1,0:T(8,128)(2,1)S(1)}, bf16[1072,128]{1,0:T(8,128)(2,1)S(1)}, u32[]{:S(2)}, u32[]{:S(2)}) collective-permute-start(bf16[1072,128]{1,0:T(8,128)(2,1)S(1)} %get-tuple-element.42), channel_id=1, source_target_pairs={{0,16},{8,24},{16,0},{24,8},{1,17},{9,25},{17,1},{25,9},{2,18},{10... | collective-permute-start | bytes 823304 | tf_op jit(solution)/shard_map/ppermute | solution.py:37
  21.1 51.1 %collective-permute-start.2 = (bf16[1072,128]{1,0:T(8,128)(2,1)S(1)}, bf16[1072,128]{1,0:T(8,128)(2,1)S(1)}, u32[]{:S(2)}, u32[]{:S(2)}) collective-permute-start(bf16[1072,128]{1,0:T(8,128)(2,1)S(1)} %get-tuple-element.41), channel_id=1, source_target_pairs={{0,24},{8,16},{16,8},{24,0},{1,25},{9,17},{17,9},{25,1},{2,26},{10... | collective-permute-start | bytes 823304 | tf_op jit(solution)/shard_map/ppermute | solution.py:37
  25.9 46.4 %collective-permute-start = (bf16[1072,128]{1,0:T(8,128)(2,1)S(1)}, bf16[1072,128]{1,0:T(8,128)(2,1)S(1)}, u32[]{:S(2)}, u32[]{:S(2)}) collective-permute-start(bf16[1072,128]{1,0:T(8,128)(2,1)S(1)} %get-tuple-element.43), channel_id=1, source_target_pairs={{0,8},{8,0},{16,24},{24,16},{1,9},{9,1},{17,25},{25,17},{2,10},{10... | collective-permute-start | bytes 823304 | tf_op jit(solution)/shard_map/ppermute | solution.py:37
  28.7 67.4 %all-to-all-start.1 = ((bf16[8,4,1408]{2,1,0:T(4,128)(2,1)}), bf16[8,4,1408]{2,1,0:T(4,128)(2,1)S(1)}, u32[]{:S(2)}, u32[]{:S(2)}) async-start(bf16[8,4,1408]{2,1,0:T(4,128)(2,1)} %reshape.210), calls=%async_computation.1 | async-start | bytes 180224 | tf_op jit(solution)/shard_map/all_to_all | solution.py:23
  73.3 23.2 %copy-start = (f32[4,8,64,128]{3,2,1,0:T(8,128)S(1)}, f32[4,8,64,128]{3,2,1,0:T(8,128)}, u32[]{:S(2)}) copy-start(f32[4,8,64,128]{3,2,1,0:T(8,128)} %param.24) | copy-start | bytes 3145732
  73.3 23.6 %copy-start.11 = (f32[8]{0:T(128)S(1)}, f32[8]{0:T(128)}, u32[]{:S(2)}) copy-start(f32[8]{0:T(128)} %param.31) | copy-start | bytes 100
  98.2 24.7 %all-to-all-start.2 = ((bf16[8,4,512]{2,1,0:T(4,128)(2,1)}), bf16[8,4,512]{2,1,0:T(4,128)(2,1)S(1)}, u32[]{:S(2)}, u32[]{:S(2)}) async-start(bf16[8,4,512]{2,1,0:T(4,128)(2,1)} %broadcast_in_dim.55), calls=%async_computation.2 | async-start | bytes 65536 | tf_op jit(solution)/shard_map/all_to_all | solution.py:28
  157.9 38.9 %copy-start.2 = (bf16[2048,128]{1,0:T(8,128)(2,1)S(1)}, bf16[2048,128]{1,0:T(8,128)(2,1)}, u32[]{:S(2)}) copy-start(bf16[2048,128]{1,0:T(8,128)(2,1)} %param.39) | copy-start | bytes 1572868
  190.3 32.6 %all-to-all-start.6 = ((bf16[8,16,512]{2,1,0:T(8,128)(2,1)}), bf16[8,16,512]{2,1,0:T(8,128)(2,1)S(1)}, u32[]{:S(2)}, u32[]{:S(2)}) async-start(bf16[8,16,512]{2,1,0:T(8,128)(2,1)} %broadcast_in_dim.71), calls=%async_computation.6 | async-start | bytes 262144 | tf_op jit(solution)/shard_map/all_to_all | solution.py:28
  196.9 16.4 %collective-permute-start.3 = (bf16[512,128]{1,0:T(8,128)(2,1)S(1)}, bf16[512,128]{1,0:T(8,128)(2,1)S(1)}, u32[]{:S(2)}, u32[]{:S(2)}) collective-permute-start(bf16[512,128]{1,0:T(8,128)(2,1)S(1)} %get-tuple-element.47), channel_id=1, source_target_pairs={{0,8},{8,0},{16,24},{24,16},{1,9},{9,1},{17,25},{25,17},{2,10},{10... | collective-permute-start | bytes 393224 | tf_op jit(solution)/shard_map/ppermute | solution.py:37
  199.7 14.1 %collective-permute-start.4 = (bf16[512,128]{1,0:T(8,128)(2,1)S(1)}, bf16[512,128]{1,0:T(8,128)(2,1)S(1)}, u32[]{:S(2)}, u32[]{:S(2)}) collective-permute-start(bf16[512,128]{1,0:T(8,128)(2,1)S(1)} %get-tuple-element.46), channel_id=1, source_target_pairs={{0,16},{8,24},{16,0},{24,8},{1,17},{9,25},{17,1},{25,9},{2,18},{10... | collective-permute-start | bytes 393224 | tf_op jit(solution)/shard_map/ppermute | solution.py:37
  203.9 15.8 %collective-permute-start.5 = (bf16[512,128]{1,0:T(8,128)(2,1)S(1)}, bf16[512,128]{1,0:T(8,128)(2,1)S(1)}, u32[]{:S(2)}, u32[]{:S(2)}) collective-permute-start(bf16[512,128]{1,0:T(8,128)(2,1)S(1)} %get-tuple-element.45), channel_id=1, source_target_pairs={{0,24},{8,16},{16,8},{24,0},{1,25},{9,17},{17,9},{25,1},{2,26},{10... | collective-permute-start | bytes 393224 | tf_op jit(solution)/shard_map/ppermute | solution.py:37
where the time goes:
time: 253 us; the launch traced here: 252 us
  blocking collectives  91.9 us (36%)
  starting transfers between devices  81.1 us (32%)
  waiting for transfers between devices  64.6 us (26%)
  local copies, waits for them, and re-layouts  4.83 us (2%)
  other arithmetic  4.18 us (2%)
    all_to_all x2, starting transfers between devices, scattered_sum(): lax.all_to_all(parts, along, 0, 0, tiled=True).astype(f32).sum(axis=0)  52.6 us
    all_to_all x3, blocking collectives, from_everyone(): return lax.all_to_all(copies, along, 0, 0, tiled=True)  51.1 us
    all_to_all x1, blocking collectives, scattered_sum(): lax.all_to_all(parts, along, 0, 0, tiled=True).astype(f32).sum(axis=0)  31.2 us
    all_to_all x2, waiting for transfers between devices, scattered_sum(): lax.all_to_all(parts, along, 0, 0, tiled=True).astype(f32).sum(axis=0)  28.2 us
    all_to_all x2, waiting for transfers between devices, from_everyone(): return lax.all_to_all(copies, along, 0, 0, tiled=True)  22.8 us
    ppermute x6, starting transfers between devices, in_turn(): piece = lax.ppermute(piece, 'near', [(i, i ^ step) for i in range(near)])  18.5 us
    ppermute x6, waiting for transfers between devices, in_turn(): piece = lax.ppermute(piece, 'near', [(i, i ^ step) for i in range(near)])  13.6 us
    all_to_all x2, starting transfers between devices, from_everyone(): return lax.all_to_all(copies, along, 0, 0, tiled=True)  10 us
  transfers between devices with their start and end apart: 10, of which 7 were waited for; matrix products, arithmetic and copies ran while one was open for 2% of the time, Pallas kernels for 0%

commit v1 on v0

--- a/solution.py
+++ b/solution.py
@@ -205,9 +205,11 @@
     gated_low = (gated_rows * inner_gain.astype(f32)).astype(bf16)
     gated_low, old_state = lax.optimization_barrier((gated_low, ssm_state))
     next_state = old_state * decay[:, :, None, None] + fed[:, :, :, None] * key_heads[:, :, None, :]
+    own_tokens = near_tokens.reshape(lax.axis_size("tp"), -1, near * width)
+    own_tokens = own_tokens[lax.axis_index("tp")]
     picks = [here == i for i in range(near)]
-    own_up, own_out, near_gain, near_tokens, next_state, picks = lax.optimization_barrier(
-        (own_up, own_out, near_gain, near_tokens, next_state, picks)
+    own_up, own_out, near_gain, own_tokens, next_state, picks = lax.optimization_barrier(
+        (own_up, own_out, near_gain, own_tokens, next_state, picks)
     )
 
     all_low = from_everyone(gated_low, "far")
@@ -215,15 +217,14 @@
     ungained = all_low.astype(f32) / inner_gain.astype(f32)
     gated_squares = hi_lo(jnp.sum(ungained * ungained, axis=1, keepdims=True))
     out_part = [product(all_low, own_out[i], bf16) for i in range(near)]
-    shared = from_everyone(jnp.concatenate([*out_part, gated_squares], axis=1), "tp")
-    shared = shared.astype(f32).sum(axis=0)
+    shared = scattered_sum(jnp.concatenate([*out_part, gated_squares], axis=1), "tp")
     gated_total = jnp.sum(shared[:, near * width :], axis=1, keepdims=True)
     residual = (
-        near_tokens.astype(f32)
+        own_tokens.astype(f32)
         + shared[:, : near * width] * lax.rsqrt(gated_total / inner + epsilon)
     ).astype(bf16)
 
-    residual = from_everyone(residual, "near")
+    residual = from_everyone(residual, ("near", "tp"))
     residual = residual.reshape(batch, near * width)
     residual_wide = residual.astype(f32)
     hidden_low = (residual_wide * near_gain).astype(bf16)

time: 253 us -> 255 us (level)
  blocking collectives: 91.9 us -> 96 us
    all_to_all x3 -> x2, blocking collectives: 51.1 us -> 35.1 us  [from_everyone(): return lax.all_to_all(copies, along, 0, 0, tiled=True)]
    all_to_all x1 -> x2, blocking collectives: 31.2 us -> 45.9 us  [scattered_sum(): lax.all_to_all(parts, along, 0, 0, tiled=True).astype(f32).sum(axis=0)]
    all_to_all x1, blocking collectives: 9.55 us -> 15 us  [per_device(): lax.all_to_all(down_part, 'near', 0, 0, tiled=True).astype(f32).sum(axis=0)]
  transfers between devices with their start and end apart: 10 -> 10, of which waited for: 7 -> 6; matrix products, arithmetic and copies ran while one was open for 2% -> 2% of each run, Pallas kernels for 0% -> 0%
where the time goes in v1:
time: 255 us
  blocking collectives  96 us (38%)
  starting transfers between devices  81.8 us (32%)
  waiting for transfers between devices  62.6 us (25%)
  local copies, waits for them, and re-layouts  4.95 us (2%)
  other arithmetic  4.2 us (2%)
    all_to_all x2, starting transfers between devices, scattered_sum(): lax.all_to_all(parts, along, 0, 0, tiled=True).astype(f32).sum(axis=0)  52.6 us
    all_to_all x2, blocking collectives, scattered_sum(): lax.all_to_all(parts, along, 0, 0, tiled=True).astype(f32).sum(axis=0)  45.9 us
    all_to_all x2, blocking collectives, from_everyone(): return lax.all_to_all(copies, along, 0, 0, tiled=True)  35.1 us
    all_to_all x2, waiting for transfers between devices, scattered_sum(): lax.all_to_all(parts, along, 0, 0, tiled=True).astype(f32).sum(axis=0)  28.1 us
    all_to_all x2, waiting for transfers between devices, from_everyone(): return lax.all_to_all(copies, along, 0, 0, tiled=True)  20.5 us
    ppermute x6, starting transfers between devices, in_turn(): piece = lax.ppermute(piece, 'near', [(i, i ^ step) for i in range(near)])  18.5 us
    all_to_all x1, blocking collectives, per_device(): lax.all_to_all(down_part, 'near', 0, 0, tiled=True).astype(f32).sum(axis=0)  15 us
    ppermute x6, waiting for transfers between devices, in_turn(): piece = lax.ppermute(piece, 'near', [(i, i ^ step) for i in range(near)])  14 us
  transfers between devices with their start and end apart: 10, of which 6 were waited for; matrix products, arithmetic and copies ran while one was open for 2% of the time, Pallas kernels for 0%

profile of v1, /device:TPU:33, one launch (start us, length us, event | category | flops | bytes accessed | tf_op | source)
XLA Modules:
  0.0 254.7 jit_solution(18013491481541764274)
XLA Ops:
  0.6 2.2 project.1
  2.9 9.0 %all-to-all-start = ((bf16[4,32,1408]{2,1,0:T(8,128)(2,1)}), bf16[4,32,1408]{2,1,0:T(8,128)(2,1)S(1)}, u32[]{:S(2)}, u32[]{:S(2)}) async-start(bf16[4,32,1408]{2,1,0:T(8,128)(2,1)} %bitcast.189), calls=%async_computation | async-start | bytes 720896 | tf_op jit(solution)/shard_map/all_to_all | solution.py:23
  12.8 5.5 %all-to-all-done = bf16[4,32,1408]{2,1,0:T(8,128)(2,1)S(1)} async-done(((bf16[4,32,1408]{2,1,0:T(8,128)(2,1)}), bf16[4,32,1408]{2,1,0:T(8,128)(2,1)S(1)}, u32[]{:S(2)}, u32[]{:S(2)}) %all-to-all-start) | async-done | bytes 360480 | tf_op jit(solution)/shard_map/all_to_all | solution.py:23
  18.7 2.4 collective-permute-start.1
  21.1 4.8 %collective-permute-start.2 = (bf16[1072,128]{1,0:T(8,128)(2,1)S(1)}, bf16[1072,128]{1,0:T(8,128)(2,1)S(1)}, u32[]{:S(2)}, u32[]{:S(2)}) collective-permute-start(bf16[1072,128]{1,0:T(8,128)(2,1)S(1)} %get-tuple-element.41), channel_id=1, source_target_pairs={{0,24},{8,16},{16,8},{24,0},{1,25},{9,17},{17,9},{25,1},{2,26},{10... | collective-permute-start | bytes 823304 | tf_op jit(solution)/shard_map/ppermute | solution.py:37
  25.9 2.0 collective-permute-start
  28.7 43.6 %all-to-all-start.1 = ((bf16[8,4,1408]{2,1,0:T(4,128)(2,1)}), bf16[8,4,1408]{2,1,0:T(4,128)(2,1)S(1)}, u32[]{:S(2)}, u32[]{:S(2)}) async-start(bf16[8,4,1408]{2,1,0:T(4,128)(2,1)} %reshape.209), calls=%async_computation.1 | async-start | bytes 180224 | tf_op jit(solution)/shard_map/all_to_all | solution.py:23
  73.4 22.6 %all-to-all-done.1 = bf16[8,4,1408]{2,1,0:T(4,128)(2,1)S(1)} async-done(((bf16[8,4,1408]{2,1,0:T(4,128)(2,1)}), bf16[8,4,1408]{2,1,0:T(4,128)(2,1)S(1)}, u32[]{:S(2)}, u32[]{:S(2)}) %all-to-all-start.1) | async-done | bytes 90144 | tf_op jit(solution)/shard_map/all_to_all | solution.py:23
  98.2 3.5 %all-to-all-start.2 = ((bf16[8,4,512]{2,1,0:T(4,128)(2,1)}), bf16[8,4,512]{2,1,0:T(4,128)(2,1)S(1)}, u32[]{:S(2)}, u32[]{:S(2)}) async-start(bf16[8,4,512]{2,1,0:T(4,128)(2,1)} %broadcast_in_dim.53), calls=%async_computation.2 | async-start | bytes 65536 | tf_op jit(solution)/shard_map/all_to_all | solution.py:28
  101.7 1.3 multiply_add_fusion
  103.1 19.8 %all-to-all-done.2 = bf16[8,4,512]{2,1,0:T(4,128)(2,1)S(1)} async-done(((bf16[8,4,512]{2,1,0:T(4,128)(2,1)}), bf16[8,4,512]{2,1,0:T(4,128)(2,1)S(1)}, u32[]{:S(2)}, u32[]{:S(2)}) %all-to-all-start.2) | async-done | bytes 32800 | tf_op jit(solution)/shard_map/all_to_all | solution.py:28
  123.9 14.3 %all_to_all.45 = bf16[8,4,640]{2,1,0:T(4,128)(2,1)S(1)} all-to-all(bf16[8,4,640]{2,1,0:T(4,128)(2,1)S(1)} %reshape.212), channel_id=1, replica_groups=mesh['grp'=2,'far'=8,'near'=4,'tp'=8] {'tp'}, dimensions={0} | all-to-all | bytes 81920 | tf_op jit(solution)/shard_map/all_to_all | solution.py:23
  138.5 22.1 %all_to_all.46 = bf16[32,4,512]{2,1,0:T(4,128)(2,1)S(1)} all-to-all(bf16[32,4,512]{2,1,0:T(4,128)(2,1)S(1)} %broadcast_in_dim.57), channel_id=1, replica_groups=mesh['grp'=2,'far'=8,'near'=4,'tp'=8] {'near','tp'}, dimensions={0} | all-to-all | bytes 262144 | tf_op jit(solution)/shard_map/all_to_all | solution.py:28
  161.3 31.6 %all_to_all.47 = bf16[8,16,640]{2,1,0:T(8,128)(2,1)S(1)} all-to-all(bf16[8,16,640]{2,1,0:T(8,128)(2,1)S(1)} %bitcast.187), channel_id=1, replica_groups=mesh['grp'=2,'far'=8,'near'=4,'tp'=8] {'far'}, dimensions={0} | all-to-all | bytes 327680 | tf_op jit(solution)/shard_map/all_to_all | solution.py:23
  193.1 0.7 broadcast_in_dim.65
  193.8 7.1 %all-to-all-start.6 = ((bf16[8,16,512]{2,1,0:T(8,128)(2,1)}), bf16[8,16,512]{2,1,0:T(8,128)(2,1)S(1)}, u32[]{:S(2)}, u32[]{:S(2)}) async-start(bf16[8,16,512]{2,1,0:T(8,128)(2,1)} %broadcast_in_dim.65), calls=%async_computation.6 | async-start | bytes 262144 | tf_op jit(solution)/shard_map/all_to_all | solution.py:28
  201.0 2.8 %collective-permute-start.3 = (bf16[512,128]{1,0:T(8,128)(2,1)S(1)}, bf16[512,128]{1,0:T(8,128)(2,1)S(1)}, u32[]{:S(2)}, u32[]{:S(2)}) collective-permute-start(bf16[512,128]{1,0:T(8,128)(2,1)S(1)} %get-tuple-element.47), channel_id=1, source_target_pairs={{0,8},{8,0},{16,24},{24,16},{1,9},{9,1},{17,25},{25,17},{2,10},{10... | collective-permute-start | bytes 393224 | tf_op jit(solution)/shard_map/ppermute | solution.py:37
  203.8 2.2 collective-permute-start.4
  206.0 4.4 %collective-permute-start.5 = (bf16[512,128]{1,0:T(8,128)(2,1)S(1)}, bf16[512,128]{1,0:T(8,128)(2,1)S(1)}, u32[]{:S(2)}, u32[]{:S(2)}) collective-permute-start(bf16[512,128]{1,0:T(8,128)(2,1)S(1)} %get-tuple-element.45), channel_id=1, source_target_pairs={{0,24},{8,16},{16,8},{24,0},{1,25},{9,17},{17,9},{25,1},{2,26},{10... | collective-permute-start | bytes 393224 | tf_op jit(solution)/shard_map/ppermute | solution.py:37
  210.4 3.7 %collective-permute-done.3 = bf16[512,128]{1,0:T(8,128)(2,1)S(1)} collective-permute-done((bf16[512,128]{1,0:T(8,128)(2,1)S(1)}, bf16[512,128]{1,0:T(8,128)(2,1)S(1)}, u32[]{:S(2)}, u32[]{:S(2)}) %collective-permute-start.3) | collective-permute-done | bytes 131104 | tf_op jit(solution)/shard_map/ppermute | solution.py:37
  214.0 10.3 %collective-permute-done.4 = bf16[512,128]{1,0:T(8,128)(2,1)S(1)} collective-permute-done((bf16[512,128]{1,0:T(8,128)(2,1)S(1)}, bf16[512,128]{1,0:T(8,128)(2,1)S(1)}, u32[]{:S(2)}, u32[]{:S(2)}) %collective-permute-start.4) | collective-permute-done | bytes 131104 | tf_op jit(solution)/shard_map/ppermute | solution.py:37
  224.4 0.7 all-to-all-done.6
  225.9 15.0 %all_to_all.48 = bf16[4,128,128]{2,1,0:T(8,128)(2,1)S(1)} all-to-all(bf16[4,128,128]{2,1,0:T(8,128)(2,1)S(1)} %pad_maximum_fusion.5), channel_id=1, replica_groups=mesh['grp'=2,'far'=8,'near'=4,'tp'=8] {'near'}, dimensions={0} | all-to-all | bytes 262144 | tf_op jit(solution)/shard_map/all_to_all | solution.py:246
  241.0 13.0 %all_to_all.49 = bf16[8,128,128]{2,1,0:T(8,128)(2,1)S(1)} all-to-all(bf16[8,128,128]{2,1,0:T(8,128)(2,1)S(1)} %broadcast_in_dim.66), channel_id=1, replica_groups=mesh['grp'=2,'far'=8,'near'=4,'tp'=8] {'tp'}, dimensions={0} | all-to-all | bytes 524288 | tf_op jit(solution)/shard_map/all_to_all | solution.py:28
  (121 shorter events, 8.7 us)
Async XLA Ops:
  0.6 11.3 %copy-start.1 = (bf16[128,2048]{1,0:T(8,128)(2,1)S(1)}, bf16[128,2048]{1,0:T(8,128)(2,1)}, u32[]{:S(2)}) copy-start(bf16[128,2048]{1,0:T(8,128)(2,1)} %param.38) | copy-start | bytes 1572868
  2.9 15.4 %all-to-all-start = ((bf16[4,32,1408]{2,1,0:T(8,128)(2,1)}), bf16[4,32,1408]{2,1,0:T(8,128)(2,1)S(1)}, u32[]{:S(2)}, u32[]{:S(2)}) async-start(bf16[4,32,1408]{2,1,0:T(8,128)(2,1)} %bitcast.189), calls=%async_computation | async-start | bytes 720896 | tf_op jit(solution)/shard_map/all_to_all | solution.py:23
  11.9 0.7 copy-start.12
  11.9 0.8 copy-start.13
  11.9 0.8 copy-start.8
  11.9 0.8 copy-start.5
  11.9 0.8 copy-start.7
  11.9 6.4 %copy-start.10 = (bf16[128]{0:T(256)(128)(2,1)S(1)}, bf16[128]{0:T(256)(128)(2,1)}, u32[]{:S(2)}) copy-start(bf16[128]{0:T(256)(128)(2,1)} %param.37) | copy-start | bytes 772
  12.0 6.5 %copy-start.3 = (bf16[512,128]{1,0:T(8,128)(2,1)S(1)}, bf16[512,128]{1,0:T(8,128)(2,1)}, u32[]{:S(2)}) copy-start(bf16[512,128]{1,0:T(8,128)(2,1)} %param.36) | copy-start | bytes 393220
  12.2 6.3 %copy-start.4 = (bf16[128,128]{1,0:T(8,128)(2,1)S(1)}, bf16[128,128]{1,0:T(8,128)(2,1)}, u32[]{:S(2)}) copy-start(bf16[128,128]{1,0:T(8,128)(2,1)} %get-tuple-element.16) | copy-start | bytes 98308
  18.6 9.3 %copy-start.9 = (bf16[512]{0:T(512)(128)(2,1)S(1)}, bf16[512]{0:T(512)(128)(2,1)}, u32[]{:S(2)}) copy-start(bf16[512]{0:T(512)(128)(2,1)} %param.35) | copy-start | bytes 3076
  18.6 9.3 %copy-start.6 = (bf16[4,3,512]{2,0,1:T(4,128)(2,1)S(1)}, bf16[4,3,512]{2,0,1:T(4,128)(2,1)}, u32[]{:S(2)}) copy-start(bf16[4,3,512]{2,0,1:T(4,128)(2,1)} %param.22) | copy-start | bytes 36868
  18.7 53.6 %collective-permute-start.1 = (bf16[1072,128]{1,0:T(8,128)(2,1)S(1)}, bf16[1072,128]{1,0:T(8,128)(2,1)S(1)}, u32[]{:S(2)}, u32[]{:S(2)}) collective-permute-start(bf16[1072,128]{1,0:T(8,128)(2,1)S(1)} %get-tuple-element.42), channel_id=1, source_target_pairs={{0,16},{8,24},{16,0},{24,8},{1,17},{9,25},{17,1},{25,9},{2,18},{10... | collective-permute-start | bytes 823304 | tf_op jit(solution)/shard_map/ppermute | solution.py:37
  21.1 51.1 %collective-permute-start.2 = (bf16[1072,128]{1,0:T(8,128)(2,1)S(1)}, bf16[1072,128]{1,0:T(8,128)(2,1)S(1)}, u32[]{:S(2)}, u32[]{:S(2)}) collective-permute-start(bf16[1072,128]{1,0:T(8,128)(2,1)S(1)} %get-tuple-element.41), channel_id=1, source_target_pairs={{0,24},{8,16},{16,8},{24,0},{1,25},{9,17},{17,9},{25,1},{2,26},{10... | collective-permute-start | bytes 823304 | tf_op jit(solution)/shard_map/ppermute | solution.py:37
  25.9 46.4 %collective-permute-start = (bf16[1072,128]{1,0:T(8,128)(2,1)S(1)}, bf16[1072,128]{1,0:T(8,128)(2,1)S(1)}, u32[]{:S(2)}, u32[]{:S(2)}) collective-permute-start(bf16[1072,128]{1,0:T(8,128)(2,1)S(1)} %get-tuple-element.43), channel_id=1, source_target_pairs={{0,8},{8,0},{16,24},{24,16},{1,9},{9,1},{17,25},{25,17},{2,10},{10... | collective-permute-start | bytes 823304 | tf_op jit(solution)/shard_map/ppermute | solution.py:37
  28.7 67.4 %all-to-all-start.1 = ((bf16[8,4,1408]{2,1,0:T(4,128)(2,1)}), bf16[8,4,1408]{2,1,0:T(4,128)(2,1)S(1)}, u32[]{:S(2)}, u32[]{:S(2)}) async-start(bf16[8,4,1408]{2,1,0:T(4,128)(2,1)} %reshape.209), calls=%async_computation.1 | async-start | bytes 180224 | tf_op jit(solution)/shard_map/all_to_all | solution.py:23
  73.3 23.3 %copy-start = (f32[4,8,64,128]{3,2,1,0:T(8,128)S(1)}, f32[4,8,64,128]{3,2,1,0:T(8,128)}, u32[]{:S(2)}) copy-start(f32[4,8,64,128]{3,2,1,0:T(8,128)} %param.24) | copy-start | bytes 3145732
  73.4 23.5 %copy-start.11 = (f32[8]{0:T(128)S(1)}, f32[8]{0:T(128)}, u32[]{:S(2)}) copy-start(f32[8]{0:T(128)} %param.31) | copy-start | bytes 100
  98.2 24.7 %all-to-all-start.2 = ((bf16[8,4,512]{2,1,0:T(4,128)(2,1)}), bf16[8,4,512]{2,1,0:T(4,128)(2,1)S(1)}, u32[]{:S(2)}, u32[]{:S(2)}) async-start(bf16[8,4,512]{2,1,0:T(4,128)(2,1)} %broadcast_in_dim.53), calls=%async_computation.2 | async-start | bytes 65536 | tf_op jit(solution)/shard_map/all_to_all | solution.py:28
  161.0 39.9 %copy-start.2 = (bf16[2048,128]{1,0:T(8,128)(2,1)S(1)}, bf16[2048,128]{1,0:T(8,128)(2,1)}, u32[]{:S(2)}) copy-start(bf16[2048,128]{1,0:T(8,128)(2,1)} %param.39) | copy-start | bytes 1572868
  193.8 31.3 %all-to-all-start.6 = ((bf16[8,16,512]{2,1,0:T(8,128)(2,1)}), bf16[8,16,512]{2,1,0:T(8,128)(2,1)S(1)}, u32[]{:S(2)}, u32[]{:S(2)}) async-start(bf16[8,16,512]{2,1,0:T(8,128)(2,1)} %broadcast_in_dim.65), calls=%async_computation.6 | async-start | bytes 262144 | tf_op jit(solution)/shard_map/all_to_all | solution.py:28
  201.0 13.0 %collective-permute-start.3 = (bf16[512,128]{1,0:T(8,128)(2,1)S(1)}, bf16[512,128]{1,0:T(8,128)(2,1)S(1)}, u32[]{:S(2)}, u32[]{:S(2)}) collective-permute-start(bf16[512,128]{1,0:T(8,128)(2,1)S(1)} %get-tuple-element.47), channel_id=1, source_target_pairs={{0,8},{8,0},{16,24},{24,16},{1,9},{9,1},{17,25},{25,17},{2,10},{10... | collective-permute-start | bytes 393224 | tf_op jit(solution)/shard_map/ppermute | solution.py:37
  203.8 20.5 %collective-permute-start.4 = (bf16[512,128]{1,0:T(8,128)(2,1)S(1)}, bf16[512,128]{1,0:T(8,128)(2,1)S(1)}, u32[]{:S(2)}, u32[]{:S(2)}) collective-permute-start(bf16[512,128]{1,0:T(8,128)(2,1)S(1)} %get-tuple-element.46), channel_id=1, source_target_pairs={{0,16},{8,24},{16,0},{24,8},{1,17},{9,25},{17,1},{25,9},{2,18},{10... | collective-permute-start | bytes 393224 | tf_op jit(solution)/shard_map/ppermute | solution.py:37
  206.0 18.3 %collective-permute-start.5 = (bf16[512,128]{1,0:T(8,128)(2,1)S(1)}, bf16[512,128]{1,0:T(8,128)(2,1)S(1)}, u32[]{:S(2)}, u32[]{:S(2)}) collective-permute-start(bf16[512,128]{1,0:T(8,128)(2,1)S(1)} %get-tuple-element.45), channel_id=1, source_target_pairs={{0,24},{8,16},{16,8},{24,0},{1,25},{9,17},{17,9},{25,1},{2,26},{10... | collective-permute-start | bytes 393224 | tf_op jit(solution)/shard_map/ppermute | solution.py:37

commit v2 on v0

--- a/solution.py
+++ b/solution.py
@@ -36,9 +36,13 @@
         if step:
             piece = lax.ppermute(piece, "near", [(i, i ^ step) for i in range(near)])
         pieces.append(piece)
+    return pieces
+
+
+def in_place(pieces, here):
     pieces = jnp.stack(pieces)
     return jnp.stack(
-        [lax.dynamic_index_in_dim(pieces, here ^ i, keepdims=False) for i in range(near)]
+        [lax.dynamic_index_in_dim(pieces, here ^ i, keepdims=False) for i in range(len(pieces))]
     )
 
 
@@ -164,7 +168,7 @@
         axis=1,
     )
     here = lax.axis_index("near")
-    swapped = in_turn(packed, here)
+    swapped = in_place(in_turn(packed, here), here)
     own_up = swapped[:, :hidden].reshape(near, blocks, width, width)
     own_up = own_up.transpose(0, 2, 1, 3).reshape(near * width, hidden)
     at = hidden + w_out.shape[0]
@@ -227,21 +231,29 @@
     residual = residual.reshape(batch, near * width)
     residual_wide = residual.astype(f32)
     hidden_low = (residual_wide * near_gain).astype(bf16)
-    row_squares = jnp.sum(residual_wide * residual_wide, axis=1, keepdims=True)
-    up_part = jnp.concatenate([product(hidden_low, own_up, bf16), hi_lo(row_squares)], axis=1)
+    row_squares = jnp.sum(residual_wide * residual_wide, axis=1)
+    chunk = batch // far
+    up_part = product(hidden_low, own_up, bf16).reshape(far, chunk, blocks, width).swapaxes(1, 2)
+    high = row_squares.astype(bf16)
+    low = (row_squares - high.astype(f32)).astype(bf16)
+    squares = jnp.concatenate([high.reshape(far, 1, chunk), low.reshape(far, 1, chunk)], axis=2)
+    squares = jnp.pad(squares, ((0, 0), (0, 7), (0, width - 2 * chunk)))
+    up_part = jnp.concatenate([up_part.reshape(far, blocks * chunk, width), squares], axis=1)
     own_rows = residual[:, :width]
     for i in range(1, near):
         own_rows = jnp.where(picks[i], residual[:, i * width : (i + 1) * width], own_rows)
     up_part, own_rows = lax.optimization_barrier((up_part, own_rows))
-    up_mine = scattered_sum(up_part, "far")
+    up_mine = lax.all_to_all(up_part, "far", 0, 0, tiled=True)
+    up_mine = up_mine.astype(f32).sum(axis=0)
     own_down = in_turn(w_down.reshape(near, hidden, width), here)
-    up_share, square_share = up_mine[:, :hidden], jnp.sum(up_mine[:, hidden:], axis=1, keepdims=True)
-    active = jnp.square(
-        jax.nn.relu(up_share * lax.rsqrt(square_share / model + epsilon))
-    ).astype(bf16)
+    up_share = up_mine[: blocks * chunk].reshape(blocks, chunk, width)
+    square_share = up_mine[blocks * chunk]
+    square_share = (square_share[:chunk] + square_share[chunk : 2 * chunk])[:, None]
+    active = jnp.square(jax.nn.relu(up_share * lax.rsqrt(square_share / model + epsilon)))
+    active = active.astype(bf16).swapaxes(0, 1).reshape(chunk, hidden)
     active = from_everyone(active, "far")
     active = active.reshape(batch, hidden)
-    down_part = jnp.stack([product(active, own_down[i], bf16) for i in range(near)])
+    down_part = in_place([product(active, piece, bf16) for piece in own_down], here)
     down_sum = lax.all_to_all(down_part, "near", 0, 0, tiled=True).astype(f32).sum(axis=0)
     down_sum = from_everyone(down_sum.astype(bf16), "tp").astype(f32).sum(axis=0)
     finished = (own_rows.astype(f32) + down_sum).astype(bf16).reshape(near, far, seqs, width)

time: 253 us -> 249 us (0.984)
  blocking collectives: 91.9 us -> 71.2 us
  starting transfers between devices: 81.1 us -> 93.3 us
  waiting for transfers between devices: 64.6 us -> 68.4 us
    all_to_all x3 -> x2, blocking collectives: 51.1 us -> 32.4 us  [from_everyone(): return lax.all_to_all(copies, along, 0, 0, tiled=True)]
    all_to_all x2 -> x3, starting transfers between devices: 10 us -> 22 us  [from_everyone(): return lax.all_to_all(copies, along, 0, 0, tiled=True)]
    all_to_all x2 -> x3, waiting for transfers between devices: 22.8 us -> 30.5 us  [from_everyone(): return lax.all_to_all(copies, along, 0, 0, tiled=True)]
    ppermute x6, waiting for transfers between devices: 13.6 us -> 9.64 us  [in_turn(): piece = lax.ppermute(piece, 'near', [(i, i ^ step) for i in range(near)])]
  transfers between devices with their start and end apart: 10 -> 11, of which waited for: 7 -> 6; matrix products, arithmetic and copies ran while one was open for 2% -> 2% of each run, Pallas kernels for 0% -> 0%
where the time goes in v2:
time: 249 us; the launch traced here: 248 us
  starting transfers between devices  93.3 us (37%)
  blocking collectives  71.2 us (29%)
  waiting for transfers between devices  68.4 us (27%)
  local copies, waits for them, and re-layouts  5.7 us (2%)
  other arithmetic  4.07 us (2%)
    all_to_all x2, starting transfers between devices, scattered_sum(): lax.all_to_all(parts, along, 0, 0, tiled=True).astype(f32).sum(axis=0)  52.6 us
    all_to_all x2, blocking collectives, from_everyone(): return lax.all_to_all(copies, along, 0, 0, tiled=True)  32.4 us
    all_to_all x3, waiting for transfers between devices, from_everyone(): return lax.all_to_all(copies, along, 0, 0, tiled=True)  30.5 us
    all_to_all x1, blocking collectives, per_device(): up_mine = lax.all_to_all(up_part, 'far', 0, 0, tiled=True)  29 us
    all_to_all x2, waiting for transfers between devices, scattered_sum(): lax.all_to_all(parts, along, 0, 0, tiled=True).astype(f32).sum(axis=0)  28.2 us
    all_to_all x3, starting transfers between devices, from_everyone(): return lax.all_to_all(copies, along, 0, 0, tiled=True)  22 us
    ppermute x6, starting transfers between devices, in_turn(): piece = lax.ppermute(piece, 'near', [(i, i ^ step) for i in range(near)])  18.8 us
    all_to_all x1, blocking collectives, per_device(): lax.all_to_all(down_part, 'near', 0, 0, tiled=True).astype(f32).sum(axis=0)  9.82 us
  transfers between devices with their start and end apart: 11, of which 6 were waited for; matrix products, arithmetic and copies ran while one was open for 2% of the time, Pallas kernels for 0%

profile of v2, /device:TPU:33, one launch (start us, length us, event | category | flops | bytes accessed | tf_op | source)
XLA Modules:
  0.0 247.8 jit_solution(1104344048257055660)
XLA Ops:
  0.6 2.2 project.1
  2.9 9.0 %all-to-all-start = ((bf16[4,32,1408]{2,1,0:T(8,128)(2,1)}), bf16[4,32,1408]{2,1,0:T(8,128)(2,1)S(1)}, u32[]{:S(2)}, u32[]{:S(2)}) async-start(bf16[4,32,1408]{2,1,0:T(8,128)(2,1)} %bitcast.209), calls=%async_computation | async-start | bytes 720896 | tf_op jit(solution)/shard_map/all_to_all | solution.py:23
  12.8 5.5 %all-to-all-done = bf16[4,32,1408]{2,1,0:T(8,128)(2,1)S(1)} async-done(((bf16[4,32,1408]{2,1,0:T(8,128)(2,1)}), bf16[4,32,1408]{2,1,0:T(8,128)(2,1)S(1)}, u32[]{:S(2)}, u32[]{:S(2)}) %all-to-all-start) | async-done | bytes 360480 | tf_op jit(solution)/shard_map/all_to_all | solution.py:23
  18.7 2.4 collective-permute-start.1
  21.1 4.8 %collective-permute-start.2 = (bf16[1072,128]{1,0:T(8,128)(2,1)S(1)}, bf16[1072,128]{1,0:T(8,128)(2,1)S(1)}, u32[]{:S(2)}, u32[]{:S(2)}) collective-permute-start(bf16[1072,128]{1,0:T(8,128)(2,1)S(1)} %get-tuple-element.43), channel_id=1, source_target_pairs={{0,24},{8,16},{16,8},{24,0},{1,25},{9,17},{17,9},{25,1},{2,26},{10... | collective-permute-start | bytes 823304 | tf_op jit(solution)/shard_map/ppermute | solution.py:37
  25.9 2.0 collective-permute-start
  28.7 43.6 %all-to-all-start.1 = ((bf16[8,4,1408]{2,1,0:T(4,128)(2,1)}), bf16[8,4,1408]{2,1,0:T(4,128)(2,1)S(1)}, u32[]{:S(2)}, u32[]{:S(2)}) async-start(bf16[8,4,1408]{2,1,0:T(4,128)(2,1)} %reshape.257), calls=%async_computation.1 | async-start | bytes 180224 | tf_op jit(solution)/shard_map/all_to_all | solution.py:23
  73.3 22.7 %all-to-all-done.1 = bf16[8,4,1408]{2,1,0:T(4,128)(2,1)S(1)} async-done(((bf16[8,4,1408]{2,1,0:T(4,128)(2,1)}), bf16[8,4,1408]{2,1,0:T(4,128)(2,1)S(1)}, u32[]{:S(2)}, u32[]{:S(2)}) %all-to-all-start.1) | async-done | bytes 90144 | tf_op jit(solution)/shard_map/all_to_all | solution.py:23
  98.2 3.5 %all-to-all-start.2 = ((bf16[8,4,512]{2,1,0:T(4,128)(2,1)}), bf16[8,4,512]{2,1,0:T(4,128)(2,1)S(1)}, u32[]{:S(2)}, u32[]{:S(2)}) async-start(bf16[8,4,512]{2,1,0:T(4,128)(2,1)} %broadcast_in_dim.35), calls=%async_computation.2 | async-start | bytes 65536 | tf_op jit(solution)/shard_map/all_to_all | solution.py:28
  101.7 1.3 multiply_add_fusion
  103.1 19.8 %all-to-all-done.2 = bf16[8,4,512]{2,1,0:T(4,128)(2,1)S(1)} async-done(((bf16[8,4,512]{2,1,0:T(4,128)(2,1)}), bf16[8,4,512]{2,1,0:T(4,128)(2,1)S(1)}, u32[]{:S(2)}, u32[]{:S(2)}) %all-to-all-start.2) | async-done | bytes 32800 | tf_op jit(solution)/shard_map/all_to_all | solution.py:28
  123.9 17.0 %all_to_all.45 = bf16[8,32,640]{2,1,0:T(8,128)(2,1)S(1)} all-to-all(bf16[8,32,640]{2,1,0:T(8,128)(2,1)S(1)} %broadcast_in_dim.39), channel_id=1, replica_groups=mesh['grp'=2,'far'=8,'near'=4,'tp'=8] {'tp'}, dimensions={0} | all-to-all | bytes 655360 | tf_op jit(solution)/shard_map/all_to_all | solution.py:28
  141.2 0.7 broadcast_in_dim.40
  141.8 11.8 %all-to-all-start.4 = ((bf16[4,32,512]{2,1,0:T(8,128)(2,1)}), bf16[4,32,512]{2,1,0:T(8,128)(2,1)S(1)}, u32[]{:S(2)}, u32[]{:S(2)}) async-start(bf16[4,32,512]{2,1,0:T(8,128)(2,1)} %broadcast_in_dim.40), calls=%async_computation.4 | async-start | bytes 262144 | tf_op jit(solution)/shard_map/all_to_all | solution.py:28
  153.9 4.6 %all-to-all-done.4 = bf16[4,32,512]{2,1,0:T(8,128)(2,1)S(1)} async-done(((bf16[4,32,512]{2,1,0:T(8,128)(2,1)}), bf16[4,32,512]{2,1,0:T(8,128)(2,1)S(1)}, u32[]{:S(2)}, u32[]{:S(2)}) %all-to-all-start.4) | async-done | bytes 131104 | tf_op jit(solution)/shard_map/all_to_all | solution.py:28
  159.1 29.0 %all_to_all.46 = bf16[8,72,128]{2,1,0:T(8,128)(2,1)S(1)} all-to-all(bf16[8,72,128]{2,1,0:T(8,128)(2,1)S(1)} %fusion.3), channel_id=1, replica_groups=mesh['grp'=2,'far'=8,'near'=4,'tp'=8] {'far'}, dimensions={0} | all-to-all | bytes 294912 | tf_op jit(solution)/shard_map/all_to_all | solution.py:246
  188.9 6.6 %all-to-all-start.6 = ((bf16[8,16,512]{2,1,0:T(8,128)(2,1)}), bf16[8,16,512]{2,1,0:T(8,128)(2,1)S(1)}, u32[]{:S(2)}, u32[]{:S(2)}) async-start(bf16[8,16,512]{2,1,0:T(8,128)(2,1)} %broadcast_in_dim.41), calls=%async_computation.6 | async-start | bytes 262144 | tf_op jit(solution)/shard_map/all_to_all | solution.py:28
  195.6 3.7 %collective-permute-start.4 = (bf16[512,128]{1,0:T(8,128)(2,1)S(1)}, bf16[512,128]{1,0:T(8,128)(2,1)S(1)}, u32[]{:S(2)}, u32[]{:S(2)}) collective-permute-start(bf16[512,128]{1,0:T(8,128)(2,1)S(1)} %get-tuple-element.48), channel_id=1, source_target_pairs={{0,16},{8,24},{16,0},{24,8},{1,17},{9,25},{17,1},{25,9},{2,18},{10... | collective-permute-start | bytes 393224 | tf_op jit(solution)/shard_map/ppermute | solution.py:37
  199.3 3.9 %collective-permute-start.3 = (bf16[512,128]{1,0:T(8,128)(2,1)S(1)}, bf16[512,128]{1,0:T(8,128)(2,1)S(1)}, u32[]{:S(2)}, u32[]{:S(2)}) collective-permute-start(bf16[512,128]{1,0:T(8,128)(2,1)S(1)} %get-tuple-element.46), channel_id=1, source_target_pairs={{0,8},{8,0},{16,24},{24,16},{1,9},{9,1},{17,25},{25,17},{2,10},{10... | collective-permute-start | bytes 393224 | tf_op jit(solution)/shard_map/ppermute | solution.py:37
  203.2 2.0 collective-permute-start.5
  205.2 9.6 %collective-permute-done.4 = bf16[512,128]{1,0:T(8,128)(2,1)S(1)} collective-permute-done((bf16[512,128]{1,0:T(8,128)(2,1)S(1)}, bf16[512,128]{1,0:T(8,128)(2,1)S(1)}, u32[]{:S(2)}, u32[]{:S(2)}) %collective-permute-start.4) | collective-permute-done | bytes 131104 | tf_op jit(solution)/shard_map/ppermute | solution.py:37
  214.8 6.2 %all-to-all-done.6 = bf16[8,16,512]{2,1,0:T(8,128)(2,1)S(1)} async-done(((bf16[8,16,512]{2,1,0:T(8,128)(2,1)}), bf16[8,16,512]{2,1,0:T(8,128)(2,1)S(1)}, u32[]{:S(2)}, u32[]{:S(2)}) %all-to-all-start.6) | async-done | bytes 131104 | tf_op jit(solution)/shard_map/all_to_all | solution.py:28
  221.9 9.8 %all_to_all.47 = bf16[4,128,128]{2,1,0:T(8,128)(2,1)S(1)} all-to-all(bf16[4,128,128]{2,1,0:T(8,128)(2,1)S(1)} %pad_maximum_fusion.4), channel_id=1, replica_groups=mesh['grp'=2,'far'=8,'near'=4,'tp'=8] {'near'}, dimensions={0} | all-to-all | bytes 262144 | tf_op jit(solution)/shard_map/all_to_all | solution.py:257
  231.7 15.4 %all_to_all.48 = bf16[8,128,128]{2,1,0:T(8,128)(2,1)S(1)} all-to-all(bf16[8,128,128]{2,1,0:T(8,128)(2,1)S(1)} %broadcast_in_dim.42), channel_id=1, replica_groups=mesh['grp'=2,'far'=8,'near'=4,'tp'=8] {'tp'}, dimensions={0} | all-to-all | bytes 524288 | tf_op jit(solution)/shard_map/all_to_all | solution.py:28
  (121 shorter events, 9.3 us)
Async XLA Ops:
  0.6 11.3 %copy-start.1 = (bf16[128,2048]{1,0:T(8,128)(2,1)S(1)}, bf16[128,2048]{1,0:T(8,128)(2,1)}, u32[]{:S(2)}) copy-start(bf16[128,2048]{1,0:T(8,128)(2,1)} %param.38) | copy-start | bytes 1572868
  2.9 15.4 %all-to-all-start = ((bf16[4,32,1408]{2,1,0:T(8,128)(2,1)}), bf16[4,32,1408]{2,1,0:T(8,128)(2,1)S(1)}, u32[]{:S(2)}, u32[]{:S(2)}) async-start(bf16[4,32,1408]{2,1,0:T(8,128)(2,1)} %bitcast.209), calls=%async_computation | async-start | bytes 720896 | tf_op jit(solution)/shard_map/all_to_all | solution.py:23
  11.9 0.8 copy-start.13
  11.9 0.8 copy-start.8
  11.9 0.8 copy-start.5
  11.9 0.8 copy-start.7
  11.9 6.4 %copy-start.10 = (bf16[128]{0:T(256)(128)(2,1)S(1)}, bf16[128]{0:T(256)(128)(2,1)}, u32[]{:S(2)}) copy-start(bf16[128]{0:T(256)(128)(2,1)} %param.37) | copy-start | bytes 772
  11.9 6.5 %copy-start.3 = (bf16[512,128]{1,0:T(8,128)(2,1)S(1)}, bf16[512,128]{1,0:T(8,128)(2,1)}, u32[]{:S(2)}) copy-start(bf16[512,128]{1,0:T(8,128)(2,1)} %param.36) | copy-start | bytes 393220
  12.2 6.3 %copy-start.4 = (bf16[128,128]{1,0:T(8,128)(2,1)S(1)}, bf16[128,128]{1,0:T(8,128)(2,1)}, u32[]{:S(2)}) copy-start(bf16[128,128]{1,0:T(8,128)(2,1)} %get-tuple-element.16) | copy-start | bytes 98308
  18.6 9.3 %copy-start.9 = (bf16[512]{0:T(512)(128)(2,1)S(1)}, bf16[512]{0:T(512)(128)(2,1)}, u32[]{:S(2)}) copy-start(bf16[512]{0:T(512)(128)(2,1)} %param.35) | copy-start | bytes 3076
  18.6 9.3 %copy-start.6 = (bf16[4,3,512]{2,0,1:T(4,128)(2,1)S(1)}, bf16[4,3,512]{2,0,1:T(4,128)(2,1)}, u32[]{:S(2)}) copy-start(bf16[4,3,512]{2,0,1:T(4,128)(2,1)} %param.22) | copy-start | bytes 36868
  18.7 53.6 %collective-permute-start.1 = (bf16[1072,128]{1,0:T(8,128)(2,1)S(1)}, bf16[1072,128]{1,0:T(8,128)(2,1)S(1)}, u32[]{:S(2)}, u32[]{:S(2)}) collective-permute-start(bf16[1072,128]{1,0:T(8,128)(2,1)S(1)} %get-tuple-element.44), channel_id=1, source_target_pairs={{0,16},{8,24},{16,0},{24,8},{1,17},{9,25},{17,1},{25,9},{2,18},{10... | collective-permute-start | bytes 823304 | tf_op jit(solution)/shard_map/ppermute | solution.py:37
  21.1 51.1 %collective-permute-start.2 = (bf16[1072,128]{1,0:T(8,128)(2,1)S(1)}, bf16[1072,128]{1,0:T(8,128)(2,1)S(1)}, u32[]{:S(2)}, u32[]{:S(2)}) collective-permute-start(bf16[1072,128]{1,0:T(8,128)(2,1)S(1)} %get-tuple-element.43), channel_id=1, source_target_pairs={{0,24},{8,16},{16,8},{24,0},{1,25},{9,17},{17,9},{25,1},{2,26},{10... | collective-permute-start | bytes 823304 | tf_op jit(solution)/shard_map/ppermute | solution.py:37
  25.9 46.4 %collective-permute-start = (bf16[1072,128]{1,0:T(8,128)(2,1)S(1)}, bf16[1072,128]{1,0:T(8,128)(2,1)S(1)}, u32[]{:S(2)}, u32[]{:S(2)}) collective-permute-start(bf16[1072,128]{1,0:T(8,128)(2,1)S(1)} %get-tuple-element.45), channel_id=1, source_target_pairs={{0,8},{8,0},{16,24},{24,16},{1,9},{9,1},{17,25},{25,17},{2,10},{10... | collective-permute-start | bytes 823304 | tf_op jit(solution)/shard_map/ppermute | solution.py:37
  28.7 67.4 %all-to-all-start.1 = ((bf16[8,4,1408]{2,1,0:T(4,128)(2,1)}), bf16[8,4,1408]{2,1,0:T(4,128)(2,1)S(1)}, u32[]{:S(2)}, u32[]{:S(2)}) async-start(bf16[8,4,1408]{2,1,0:T(4,128)(2,1)} %reshape.257), calls=%async_computation.1 | async-start | bytes 180224 | tf_op jit(solution)/shard_map/all_to_all | solution.py:23
  73.3 23.2 %copy-start = (f32[4,8,64,128]{3,2,1,0:T(8,128)S(1)}, f32[4,8,64,128]{3,2,1,0:T(8,128)}, u32[]{:S(2)}) copy-start(f32[4,8,64,128]{3,2,1,0:T(8,128)} %param.24) | copy-start | bytes 3145732
  73.3 23.6 %copy-start.11 = (f32[8]{0:T(128)S(1)}, f32[8]{0:T(128)}, u32[]{:S(2)}) copy-start(f32[8]{0:T(128)} %param.31) | copy-start | bytes 100
  98.2 24.7 %all-to-all-start.2 = ((bf16[8,4,512]{2,1,0:T(4,128)(2,1)}), bf16[8,4,512]{2,1,0:T(4,128)(2,1)S(1)}, u32[]{:S(2)}, u32[]{:S(2)}) async-start(bf16[8,4,512]{2,1,0:T(4,128)(2,1)} %broadcast_in_dim.35), calls=%async_computation.2 | async-start | bytes 65536 | tf_op jit(solution)/shard_map/all_to_all | solution.py:28
  141.8 16.6 %all-to-all-start.4 = ((bf16[4,32,512]{2,1,0:T(8,128)(2,1)}), bf16[4,32,512]{2,1,0:T(8,128)(2,1)S(1)}, u32[]{:S(2)}, u32[]{:S(2)}) async-start(bf16[4,32,512]{2,1,0:T(8,128)(2,1)} %broadcast_in_dim.40), calls=%async_computation.4 | async-start | bytes 262144 | tf_op jit(solution)/shard_map/all_to_all | solution.py:28
  158.7 36.8 %copy-start.2 = (bf16[2048,128]{1,0:T(8,128)(2,1)S(1)}, bf16[2048,128]{1,0:T(8,128)(2,1)}, u32[]{:S(2)}) copy-start(bf16[2048,128]{1,0:T(8,128)(2,1)} %param.39) | copy-start | bytes 1572868
  188.9 32.1 %all-to-all-start.6 = ((bf16[8,16,512]{2,1,0:T(8,128)(2,1)}), bf16[8,16,512]{2,1,0:T(8,128)(2,1)S(1)}, u32[]{:S(2)}, u32[]{:S(2)}) async-start(bf16[8,16,512]{2,1,0:T(8,128)(2,1)} %broadcast_in_dim.41), calls=%async_computation.6 | async-start | bytes 262144 | tf_op jit(solution)/shard_map/all_to_all | solution.py:28
  195.6 19.3 %collective-permute-start.4 = (bf16[512,128]{1,0:T(8,128)(2,1)S(1)}, bf16[512,128]{1,0:T(8,128)(2,1)S(1)}, u32[]{:S(2)}, u32[]{:S(2)}) collective-permute-start(bf16[512,128]{1,0:T(8,128)(2,1)S(1)} %get-tuple-element.48), channel_id=1, source_target_pairs={{0,16},{8,24},{16,0},{24,8},{1,17},{9,25},{17,1},{25,9},{2,18},{10... | collective-permute-start | bytes 393224 | tf_op jit(solution)/shard_map/ppermute | solution.py:37
  199.3 22.1 %collective-permute-start.3 = (bf16[512,128]{1,0:T(8,128)(2,1)S(1)}, bf16[512,128]{1,0:T(8,128)(2,1)S(1)}, u32[]{:S(2)}, u32[]{:S(2)}) collective-permute-start(bf16[512,128]{1,0:T(8,128)(2,1)S(1)} %get-tuple-element.46), channel_id=1, source_target_pairs={{0,8},{8,0},{16,24},{24,16},{1,9},{9,1},{17,25},{25,17},{2,10},{10... | collective-permute-start | bytes 393224 | tf_op jit(solution)/shard_map/ppermute | solution.py:37
  203.2 18.3 %collective-permute-start.5 = (bf16[512,128]{1,0:T(8,128)(2,1)S(1)}, bf16[512,128]{1,0:T(8,128)(2,1)S(1)}, u32[]{:S(2)}, u32[]{:S(2)}) collective-permute-start(bf16[512,128]{1,0:T(8,128)(2,1)S(1)} %get-tuple-element.47), channel_id=1, source_target_pairs={{0,24},{8,16},{16,8},{24,0},{1,25},{9,17},{17,9},{25,1},{2,26},{10... | collective-permute-start | bytes 393224 | tf_op jit(solution)/shard_map/ppermute | solution.py:37
  (1 other events, 0.7 us)

commit v3 on v2

--- a/solution.py
+++ b/solution.py
@@ -208,10 +208,11 @@
     gated_rows = mixer_y * jax.nn.silu(gate_raw * inverse)
     gated_low = (gated_rows * inner_gain.astype(f32)).astype(bf16)
     gated_low, old_state = lax.optimization_barrier((gated_low, ssm_state))
-    next_state = old_state * decay[:, :, None, None] + fed[:, :, :, None] * key_heads[:, :, None, :]
+    added = fed[:, :, :, None] * key_heads[:, :, None, :]
+    next_state = old_state * decay[:, :, None, None] + added
     picks = [here == i for i in range(near)]
-    own_up, own_out, near_gain, near_tokens, next_state, picks = lax.optimization_barrier(
-        (own_up, own_out, near_gain, near_tokens, next_state, picks)
+    own_up, own_out, near_gain, near_tokens, picks = lax.optimization_barrier(
+        (own_up, own_out, near_gain, near_tokens, picks)
     )
 
     all_low = from_everyone(gated_low, "far")

time: 249 us -> 251 us (level)
  blocking collectives: 71.2 us -> 46 us
  starting transfers between devices: 93.3 us -> 108 us
  waiting for transfers between devices: 68.4 us -> 78.8 us
    all_to_all x2 -> x1, blocking collectives: 32.4 us -> 17 us  [from_everyone(): return lax.all_to_all(copies, along, 0, 0, tiled=True)]
    all_to_all x3 -> x4, starting transfers between devices: 22 us -> 31.8 us  [from_everyone(): return lax.all_to_all(copies, along, 0, 0, tiled=True)]
    all_to_all x1 -> x0, blocking collectives: 9.82 us -> none  [per_device(): lax.all_to_all(down_part, 'near', 0, 0, tiled=True).astype(f32).sum(axis=0)]
    all_to_all x0 -> x1, starting transfers between devices: none -> 5.24 us  [per_device(): lax.all_to_all(down_part, 'near', 0, 0, tiled=True).astype(f32).sum(axis=0)]
    all_to_all x3 -> x4, waiting for transfers between devices: 30.5 us -> 35.7 us  [from_everyone(): return lax.all_to_all(copies, along, 0, 0, tiled=True)]
    all_to_all x0 -> x1, waiting for transfers between devices: none -> 4.62 us  [per_device(): lax.all_to_all(down_part, 'near', 0, 0, tiled=True).astype(f32).sum(axis=0)]
  transfers between devices with their start and end apart: 11 -> 13, of which waited for: 6 -> 8; matrix products, arithmetic and copies ran while one was open for 2% -> 2% of each run, Pallas kernels for 0% -> 0%
where the time goes in v3:
time: 251 us; the launch traced here: 250 us
  starting transfers between devices  108 us (43%)
  waiting for transfers between devices  78.8 us (31%)
  blocking collectives  46 us (18%)
  local copies, waits for them, and re-layouts  7.23 us (3%)
  other arithmetic  4.72 us (2%)
    all_to_all x2, starting transfers between devices, scattered_sum(): lax.all_to_all(parts, along, 0, 0, tiled=True).astype(f32).sum(axis=0)  52.6 us
    all_to_all x4, waiting for transfers between devices, from_everyone(): return lax.all_to_all(copies, along, 0, 0, tiled=True)  35.7 us
    all_to_all x4, starting transfers between devices, from_everyone(): return lax.all_to_all(copies, along, 0, 0, tiled=True)  31.8 us
    all_to_all x1, blocking collectives, per_device(): up_mine = lax.all_to_all(up_part, 'far', 0, 0, tiled=True)  29 us
    all_to_all x2, waiting for transfers between devices, scattered_sum(): lax.all_to_all(parts, along, 0, 0, tiled=True).astype(f32).sum(axis=0)  28.8 us
    ppermute x6, starting transfers between devices, in_turn(): piece = lax.ppermute(piece, 'near', [(i, i ^ step) for i in range(near)])  18.8 us
    all_to_all x1, blocking collectives, from_everyone(): return lax.all_to_all(copies, along, 0, 0, tiled=True)  17 us
    ppermute x6, waiting for transfers between devices, in_turn(): piece = lax.ppermute(piece, 'near', [(i, i ^ step) for i in range(near)])  9.64 us
  transfers between devices with their start and end apart: 13, of which 8 were waited for; matrix products, arithmetic and copies ran while one was open for 2% of the time, Pallas kernels for 0%

profile of v3, /device:TPU:33, one launch (start us, length us, event | category | flops | bytes accessed | tf_op | source)
XLA Modules:
  0.0 250.3 jit_solution(3246367317059094754)
XLA Ops:
  0.6 2.2 project.1
  2.9 9.0 %all-to-all-start = ((bf16[4,32,1408]{2,1,0:T(8,128)(2,1)}), bf16[4,32,1408]{2,1,0:T(8,128)(2,1)S(1)}, u32[]{:S(2)}, u32[]{:S(2)}) async-start(bf16[4,32,1408]{2,1,0:T(8,128)(2,1)} %bitcast.209), calls=%async_computation | async-start | bytes 720896 | tf_op jit(solution)/shard_map/all_to_all | solution.py:23
  12.8 5.5 %all-to-all-done = bf16[4,32,1408]{2,1,0:T(8,128)(2,1)S(1)} async-done(((bf16[4,32,1408]{2,1,0:T(8,128)(2,1)}), bf16[4,32,1408]{2,1,0:T(8,128)(2,1)S(1)}, u32[]{:S(2)}, u32[]{:S(2)}) %all-to-all-start) | async-done | bytes 360480 | tf_op jit(solution)/shard_map/all_to_all | solution.py:23
  18.7 2.4 collective-permute-start.1
  21.1 4.8 %collective-permute-start.2 = (bf16[1072,128]{1,0:T(8,128)(2,1)S(1)}, bf16[1072,128]{1,0:T(8,128)(2,1)S(1)}, u32[]{:S(2)}, u32[]{:S(2)}) collective-permute-start(bf16[1072,128]{1,0:T(8,128)(2,1)S(1)} %get-tuple-element.41), channel_id=1, source_target_pairs={{0,24},{8,16},{16,8},{24,0},{1,25},{9,17},{17,9},{25,1},{2,26},{10... | collective-permute-start | bytes 823304 | tf_op jit(solution)/shard_map/ppermute | solution.py:37
  25.9 2.0 collective-permute-start
  28.7 43.6 %all-to-all-start.1 = ((bf16[8,4,1408]{2,1,0:T(4,128)(2,1)}), bf16[8,4,1408]{2,1,0:T(4,128)(2,1)S(1)}, u32[]{:S(2)}, u32[]{:S(2)}) async-start(bf16[8,4,1408]{2,1,0:T(4,128)(2,1)} %reshape.257), calls=%async_computation.1 | async-start | bytes 180224 | tf_op jit(solution)/shard_map/all_to_all | solution.py:23
  72.7 23.3 %all-to-all-done.1 = bf16[8,4,1408]{2,1,0:T(4,128)(2,1)S(1)} async-done(((bf16[8,4,1408]{2,1,0:T(4,128)(2,1)}), bf16[8,4,1408]{2,1,0:T(4,128)(2,1)S(1)}, u32[]{:S(2)}, u32[]{:S(2)}) %all-to-all-start.1) | async-done | bytes 90144 | tf_op jit(solution)/shard_map/all_to_all | solution.py:23
  98.0 3.5 %all-to-all-start.2 = ((bf16[8,4,512]{2,1,0:T(4,128)(2,1)}), bf16[8,4,512]{2,1,0:T(4,128)(2,1)S(1)}, u32[]{:S(2)}, u32[]{:S(2)}) async-start(bf16[8,4,512]{2,1,0:T(4,128)(2,1)} %broadcast_in_dim.35), calls=%async_computation.2 | async-start | bytes 65536 | tf_op jit(solution)/shard_map/all_to_all | solution.py:28
  103.0 19.7 %all-to-all-done.2 = bf16[8,4,512]{2,1,0:T(4,128)(2,1)S(1)} async-done(((bf16[8,4,512]{2,1,0:T(4,128)(2,1)}), bf16[8,4,512]{2,1,0:T(4,128)(2,1)S(1)}, u32[]{:S(2)}, u32[]{:S(2)}) %all-to-all-start.2) | async-done | bytes 32800 | tf_op jit(solution)/shard_map/all_to_all | solution.py:28
  123.7 17.0 %all_to_all.45 = bf16[8,32,640]{2,1,0:T(8,128)(2,1)S(1)} all-to-all(bf16[8,32,640]{2,1,0:T(8,128)(2,1)S(1)} %broadcast_in_dim.39), channel_id=1, replica_groups=mesh['grp'=2,'far'=8,'near'=4,'tp'=8] {'tp'}, dimensions={0} | all-to-all | bytes 655360 | tf_op jit(solution)/shard_map/all_to_all | solution.py:28
  141.7 11.8 %all-to-all-start.4 = ((bf16[4,32,512]{2,1,0:T(8,128)(2,1)}), bf16[4,32,512]{2,1,0:T(8,128)(2,1)S(1)}, u32[]{:S(2)}, u32[]{:S(2)}) async-start(bf16[4,32,512]{2,1,0:T(8,128)(2,1)} %broadcast_in_dim.40), calls=%async_computation.4 | async-start | bytes 262144 | tf_op jit(solution)/shard_map/all_to_all | solution.py:28
  153.8 4.6 %all-to-all-done.4 = bf16[4,32,512]{2,1,0:T(8,128)(2,1)S(1)} async-done(((bf16[4,32,512]{2,1,0:T(8,128)(2,1)}), bf16[4,32,512]{2,1,0:T(8,128)(2,1)S(1)}, u32[]{:S(2)}, u32[]{:S(2)}) %all-to-all-start.4) | async-done | bytes 131104 | tf_op jit(solution)/shard_map/all_to_all | solution.py:28
  159.0 29.0 %all_to_all.46 = bf16[8,72,128]{2,1,0:T(8,128)(2,1)S(1)} all-to-all(bf16[8,72,128]{2,1,0:T(8,128)(2,1)S(1)} %fusion.3), channel_id=1, replica_groups=mesh['grp'=2,'far'=8,'near'=4,'tp'=8] {'far'}, dimensions={0} | all-to-all | bytes 294912 | tf_op jit(solution)/shard_map/all_to_all | solution.py:247
  188.8 6.6 %all-to-all-start.6 = ((bf16[8,16,512]{2,1,0:T(8,128)(2,1)}), bf16[8,16,512]{2,1,0:T(8,128)(2,1)S(1)}, u32[]{:S(2)}, u32[]{:S(2)}) async-start(bf16[8,16,512]{2,1,0:T(8,128)(2,1)} %broadcast_in_dim.41), calls=%async_computation.6 | async-start | bytes 262144 | tf_op jit(solution)/shard_map/all_to_all | solution.py:28
  195.4 3.7 %collective-permute-start.4 = (bf16[512,128]{1,0:T(8,128)(2,1)S(1)}, bf16[512,128]{1,0:T(8,128)(2,1)S(1)}, u32[]{:S(2)}, u32[]{:S(2)}) collective-permute-start(bf16[512,128]{1,0:T(8,128)(2,1)S(1)} %get-tuple-element.46), channel_id=1, source_target_pairs={{0,16},{8,24},{16,0},{24,8},{1,17},{9,25},{17,1},{25,9},{2,18},{10... | collective-permute-start | bytes 393224 | tf_op jit(solution)/shard_map/ppermute | solution.py:37
  199.2 3.9 %collective-permute-start.3 = (bf16[512,128]{1,0:T(8,128)(2,1)S(1)}, bf16[512,128]{1,0:T(8,128)(2,1)S(1)}, u32[]{:S(2)}, u32[]{:S(2)}) collective-permute-start(bf16[512,128]{1,0:T(8,128)(2,1)S(1)} %get-tuple-element.44), channel_id=1, source_target_pairs={{0,8},{8,0},{16,24},{24,16},{1,9},{9,1},{17,25},{25,17},{2,10},{10... | collective-permute-start | bytes 393224 | tf_op jit(solution)/shard_map/ppermute | solution.py:37
  203.1 2.0 collective-permute-start.5
  205.1 9.6 %collective-permute-done.4 = bf16[512,128]{1,0:T(8,128)(2,1)S(1)} collective-permute-done((bf16[512,128]{1,0:T(8,128)(2,1)S(1)}, bf16[512,128]{1,0:T(8,128)(2,1)S(1)}, u32[]{:S(2)}, u32[]{:S(2)}) %collective-permute-start.4) | collective-permute-done | bytes 131104 | tf_op jit(solution)/shard_map/ppermute | solution.py:37
  214.7 6.2 %all-to-all-done.6 = bf16[8,16,512]{2,1,0:T(8,128)(2,1)S(1)} async-done(((bf16[8,16,512]{2,1,0:T(8,128)(2,1)}), bf16[8,16,512]{2,1,0:T(8,128)(2,1)S(1)}, u32[]{:S(2)}, u32[]{:S(2)}) %all-to-all-start.6) | async-done | bytes 131104 | tf_op jit(solution)/shard_map/all_to_all | solution.py:28
  222.4 5.2 %all-to-all-start.7 = ((bf16[4,128,128]{2,1,0:T(8,128)(2,1)}), bf16[4,128,128]{2,1,0:T(8,128)(2,1)S(1)}, u32[]{:S(2)}, u32[]{:S(2)}) async-start(bf16[4,128,128]{2,1,0:T(8,128)(2,1)} %pad_maximum_fusion.4), calls=%async_computation.7 | async-start | bytes 262144 | tf_op jit(solution)/shard_map/all_to_all | solution.py:258
  227.8 4.6 %all-to-all-done.7 = bf16[4,128,128]{2,1,0:T(8,128)(2,1)S(1)} async-done(((bf16[4,128,128]{2,1,0:T(8,128)(2,1)}), bf16[4,128,128]{2,1,0:T(8,128)(2,1)S(1)}, u32[]{:S(2)}, u32[]{:S(2)}) %all-to-all-start.7) | async-done | bytes 131104 | tf_op jit(solution)/shard_map/all_to_all | solution.py:258
  233.2 9.9 %all-to-all-start.8 = ((bf16[8,128,128]{2,1,0:T(8,128)(2,1)}), bf16[8,128,128]{2,1,0:T(8,128)(2,1)S(1)}, u32[]{:S(2)}, u32[]{:S(2)}) async-start(bf16[8,128,128]{2,1,0:T(8,128)(2,1)} %broadcast_in_dim.42), calls=%async_computation.8 | async-start | bytes 524288 | tf_op jit(solution)/shard_map/all_to_all | solution.py:28
  244.4 5.2 %all-to-all-done.8 = bf16[8,128,128]{2,1,0:T(8,128)(2,1)S(1)} async-done(((bf16[8,128,128]{2,1,0:T(8,128)(2,1)}), bf16[8,128,128]{2,1,0:T(8,128)(2,1)S(1)}, u32[]{:S(2)}, u32[]{:S(2)}) %all-to-all-start.8) | async-done | bytes 262176 | tf_op jit(solution)/shard_map/all_to_all | solution.py:28
  (125 shorter events, 13.5 us)
Async XLA Ops:
  0.6 11.3 %copy-start.2 = (bf16[128,2048]{1,0:T(8,128)(2,1)S(1)}, bf16[128,2048]{1,0:T(8,128)(2,1)}, u32[]{:S(2)}) copy-start(bf16[128,2048]{1,0:T(8,128)(2,1)} %param.38) | copy-start | bytes 1572868
  2.9 15.4 %all-to-all-start = ((bf16[4,32,1408]{2,1,0:T(8,128)(2,1)}), bf16[4,32,1408]{2,1,0:T(8,128)(2,1)S(1)}, u32[]{:S(2)}, u32[]{:S(2)}) async-start(bf16[4,32,1408]{2,1,0:T(8,128)(2,1)} %bitcast.209), calls=%async_computation | async-start | bytes 720896 | tf_op jit(solution)/shard_map/all_to_all | solution.py:23
  11.9 0.8 copy-start.8
  11.9 6.4 %copy-start.11 = (bf16[128]{0:T(256)(128)(2,1)S(1)}, bf16[128]{0:T(256)(128)(2,1)}, u32[]{:S(2)}) copy-start(bf16[128]{0:T(256)(128)(2,1)} %param.37) | copy-start | bytes 772
  11.9 6.5 %copy-start.4 = (bf16[512,128]{1,0:T(8,128)(2,1)S(1)}, bf16[512,128]{1,0:T(8,128)(2,1)}, u32[]{:S(2)}) copy-start(bf16[512,128]{1,0:T(8,128)(2,1)} %param.36) | copy-start | bytes 393220
  12.2 6.3 %copy-start.5 = (bf16[128,128]{1,0:T(8,128)(2,1)S(1)}, bf16[128,128]{1,0:T(8,128)(2,1)}, u32[]{:S(2)}) copy-start(bf16[128,128]{1,0:T(8,128)(2,1)} %get-tuple-element.15) | copy-start | bytes 98308
  18.6 9.3 %copy-start.10 = (bf16[512]{0:T(512)(128)(2,1)S(1)}, bf16[512]{0:T(512)(128)(2,1)}, u32[]{:S(2)}) copy-start(bf16[512]{0:T(512)(128)(2,1)} %param.35) | copy-start | bytes 3076
  18.6 9.3 %copy-start.7 = (bf16[4,3,512]{2,0,1:T(4,128)(2,1)S(1)}, bf16[4,3,512]{2,0,1:T(4,128)(2,1)}, u32[]{:S(2)}) copy-start(bf16[4,3,512]{2,0,1:T(4,128)(2,1)} %param.22) | copy-start | bytes 36868
  18.7 53.6 %collective-permute-start.1 = (bf16[1072,128]{1,0:T(8,128)(2,1)S(1)}, bf16[1072,128]{1,0:T(8,128)(2,1)S(1)}, u32[]{:S(2)}, u32[]{:S(2)}) collective-permute-start(bf16[1072,128]{1,0:T(8,128)(2,1)S(1)} %get-tuple-element.42), channel_id=1, source_target_pairs={{0,16},{8,24},{16,0},{24,8},{1,17},{9,25},{17,1},{25,9},{2,18},{10... | collective-permute-start | bytes 823304 | tf_op jit(solution)/shard_map/ppermute | solution.py:37
  21.1 51.1 %collective-permute-start.2 = (bf16[1072,128]{1,0:T(8,128)(2,1)S(1)}, bf16[1072,128]{1,0:T(8,128)(2,1)S(1)}, u32[]{:S(2)}, u32[]{:S(2)}) collective-permute-start(bf16[1072,128]{1,0:T(8,128)(2,1)S(1)} %get-tuple-element.41), channel_id=1, source_target_pairs={{0,24},{8,16},{16,8},{24,0},{1,25},{9,17},{17,9},{25,1},{2,26},{10... | collective-permute-start | bytes 823304 | tf_op jit(solution)/shard_map/ppermute | solution.py:37
  25.9 46.4 %collective-permute-start = (bf16[1072,128]{1,0:T(8,128)(2,1)S(1)}, bf16[1072,128]{1,0:T(8,128)(2,1)S(1)}, u32[]{:S(2)}, u32[]{:S(2)}) collective-permute-start(bf16[1072,128]{1,0:T(8,128)(2,1)S(1)} %get-tuple-element.43), channel_id=1, source_target_pairs={{0,8},{8,0},{16,24},{24,16},{1,9},{9,1},{17,25},{25,17},{2,10},{10... | collective-permute-start | bytes 823304 | tf_op jit(solution)/shard_map/ppermute | solution.py:37
  28.7 67.4 %all-to-all-start.1 = ((bf16[8,4,1408]{2,1,0:T(4,128)(2,1)}), bf16[8,4,1408]{2,1,0:T(4,128)(2,1)S(1)}, u32[]{:S(2)}, u32[]{:S(2)}) async-start(bf16[8,4,1408]{2,1,0:T(4,128)(2,1)} %reshape.257), calls=%async_computation.1 | async-start | bytes 180224 | tf_op jit(solution)/shard_map/all_to_all | solution.py:23
  72.5 24.0 %copy-start = (f32[4,8,64,128]{3,2,1,0:T(8,128)S(1)}, f32[4,8,64,128]{3,2,1,0:T(8,128)}, u32[]{:S(2)}) copy-start(f32[4,8,64,128]{3,2,1,0:T(8,128)} %param.24) | copy-start | bytes 3145732
  72.7 24.2 %copy-start.12 = (f32[8]{0:T(128)S(1)}, f32[8]{0:T(128)}, u32[]{:S(2)}) copy-start(f32[8]{0:T(128)} %param.31) | copy-start | bytes 100
  98.0 24.7 %all-to-all-start.2 = ((bf16[8,4,512]{2,1,0:T(4,128)(2,1)}), bf16[8,4,512]{2,1,0:T(4,128)(2,1)S(1)}, u32[]{:S(2)}, u32[]{:S(2)}) async-start(bf16[8,4,512]{2,1,0:T(4,128)(2,1)} %broadcast_in_dim.35), calls=%async_computation.2 | async-start | bytes 65536 | tf_op jit(solution)/shard_map/all_to_all | solution.py:28
  102.9 19.8 %copy-start.1 = (bf16[4,512,128]{2,1,0:T(8,128)(2,1)S(1)}, bf16[4,512,128]{2,1,0:T(8,128)(2,1)}, u32[]{:S(2)}) copy-start(bf16[4,512,128]{2,1,0:T(8,128)(2,1)} %get-tuple-element.19) | copy-start | bytes 1572868
  141.7 16.6 %all-to-all-start.4 = ((bf16[4,32,512]{2,1,0:T(8,128)(2,1)}), bf16[4,32,512]{2,1,0:T(8,128)(2,1)S(1)}, u32[]{:S(2)}, u32[]{:S(2)}) async-start(bf16[4,32,512]{2,1,0:T(8,128)(2,1)} %broadcast_in_dim.40), calls=%async_computation.4 | async-start | bytes 262144 | tf_op jit(solution)/shard_map/all_to_all | solution.py:28
  158.6 36.8 %copy-start.3 = (bf16[2048,128]{1,0:T(8,128)(2,1)S(1)}, bf16[2048,128]{1,0:T(8,128)(2,1)}, u32[]{:S(2)}) copy-start(bf16[2048,128]{1,0:T(8,128)(2,1)} %param.39) | copy-start | bytes 1572868
  188.8 32.1 %all-to-all-start.6 = ((bf16[8,16,512]{2,1,0:T(8,128)(2,1)}), bf16[8,16,512]{2,1,0:T(8,128)(2,1)S(1)}, u32[]{:S(2)}, u32[]{:S(2)}) async-start(bf16[8,16,512]{2,1,0:T(8,128)(2,1)} %broadcast_in_dim.41), calls=%async_computation.6 | async-start | bytes 262144 | tf_op jit(solution)/shard_map/all_to_all | solution.py:28
  195.4 19.3 %collective-permute-start.4 = (bf16[512,128]{1,0:T(8,128)(2,1)S(1)}, bf16[512,128]{1,0:T(8,128)(2,1)S(1)}, u32[]{:S(2)}, u32[]{:S(2)}) collective-permute-start(bf16[512,128]{1,0:T(8,128)(2,1)S(1)} %get-tuple-element.46), channel_id=1, source_target_pairs={{0,16},{8,24},{16,0},{24,8},{1,17},{9,25},{17,1},{25,9},{2,18},{10... | collective-permute-start | bytes 393224 | tf_op jit(solution)/shard_map/ppermute | solution.py:37
  199.2 22.1 %collective-permute-start.3 = (bf16[512,128]{1,0:T(8,128)(2,1)S(1)}, bf16[512,128]{1,0:T(8,128)(2,1)S(1)}, u32[]{:S(2)}, u32[]{:S(2)}) collective-permute-start(bf16[512,128]{1,0:T(8,128)(2,1)S(1)} %get-tuple-element.44), channel_id=1, source_target_pairs={{0,8},{8,0},{16,24},{24,16},{1,9},{9,1},{17,25},{25,17},{2,10},{10... | collective-permute-start | bytes 393224 | tf_op jit(solution)/shard_map/ppermute | solution.py:37
  203.1 18.3 %collective-permute-start.5 = (bf16[512,128]{1,0:T(8,128)(2,1)S(1)}, bf16[512,128]{1,0:T(8,128)(2,1)S(1)}, u32[]{:S(2)}, u32[]{:S(2)}) collective-permute-start(bf16[512,128]{1,0:T(8,128)(2,1)S(1)} %get-tuple-element.45), channel_id=1, source_target_pairs={{0,24},{8,16},{16,8},{24,0},{1,25},{9,17},{17,9},{25,1},{2,26},{10... | collective-permute-start | bytes 393224 | tf_op jit(solution)/shard_map/ppermute | solution.py:37
  222.4 10.0 %all-to-all-start.7 = ((bf16[4,128,128]{2,1,0:T(8,128)(2,1)}), bf16[4,128,128]{2,1,0:T(8,128)(2,1)S(1)}, u32[]{:S(2)}, u32[]{:S(2)}) async-start(bf16[4,128,128]{2,1,0:T(8,128)(2,1)} %pad_maximum_fusion.4), calls=%async_computation.7 | async-start | bytes 262144 | tf_op jit(solution)/shard_map/all_to_all | solution.py:258
  233.2 16.4 %all-to-all-start.8 = ((bf16[8,128,128]{2,1,0:T(8,128)(2,1)}), bf16[8,128,128]{2,1,0:T(8,128)(2,1)S(1)}, u32[]{:S(2)}, u32[]{:S(2)}) async-start(bf16[8,128,128]{2,1,0:T(8,128)(2,1)} %broadcast_in_dim.42), calls=%async_computation.8 | async-start | bytes 524288 | tf_op jit(solution)/shard_map/all_to_all | solution.py:28
  (4 other events, 3.0 us)
